TPU v7x, 32 devices: a whole 2x2x4 slice. The times are simulated.
32 devices in a mesh: sp: 8 (over z, x), tp: 4 (over y, core).
Axes of the slice: x: 2, y: 2, z: 4, core: 2. Of those that a mesh axis runs over, the one named last changes fastest.
Arguments:
- mixer_in: bfloat16 [2048, 2048], P('sp', 'tp'), may hold values from -6 to 6
- doc_ids: int32 [2048], P('sp'), may hold values from 0 to 3, never falling along the last dimension, each value on 1 to 1024 neighbouring positions
- mix_scale: float32 [2048], P('tp'), may hold values from 0.1 to 1.9
- out_proj: bfloat16 [2048, 2048], P('tp'), may hold values from -0.125 to 0.125
- residual: bfloat16 [2048, 2048], P('sp'), may hold values from -6 to 6
- mix_gain: float32 [2048], replicated, may hold values from 0.1 to 1.9
- expert_ids: int32 [2048, 2], P('sp'), may hold values from 0 to 7, all different within a row; in each aligned block of 256 rows (0 to 255, 256 to 511, ...) at most 128 rows name the same one
- expert_weight: float32 [2048, 2], P('sp'), may hold values from 0.2 to 1
- w_gate: bfloat16 [8, 2048, 5632], P('sp', None, 'tp'), may hold values from -0.125 to 0.125
- w_up: bfloat16 [8, 2048, 5632], P('sp', None, 'tp'), may hold values from -0.125 to 0.125
- w_down: bfloat16 [8, 5632, 2048], P('sp', 'tp'), may hold values from -0.078125 to 0.078125
- out_gain: float32 [2048], replicated, may hold values from 0.1 to 1.9
Outputs:
- layer_out: bfloat16 [2048, 2048], P('sp')
Inputs may be any that keep to these rules, and one draw needn't show every extreme that they name: `doc_ids`: document numbers never fall along the tokens; a document has at most 1024 positions. `expert_ids`: A row's two experts differ. In each aligned block of 256 rows (the tokens of one index of sp) no expert is named by more than 128 rows; some block has an expert named by exactly 128 rows.
All inputs are finite; a program needn't handle non-finite values.
Results may differ from a plain program's by a relative error of at most 0.015.
Values may be sent and summed in bfloat16 or wider, within the bound.
A program may use at most 64 MiB of HBM per device.

v0:
```python
import jax
import jax.numpy as jnp
from jax import lax
from jax.sharding import PartitionSpec as P

alpha_res = 1.4142135623730951
norm_eps = 1e-05
pool_reach = 15


def passed_along(value, axis, steps):
    count = lax.axis_size(axis)
    initial, last = (max(0, -steps), min(count, count - steps))
    return lax.ppermute(value, axis, [(source, source + steps) for source in range(initial, last)])


def layer_norm(summed, norm_gain):
    row_mean = jnp.mean(summed, axis=-1, keepdims=True)
    centred = summed - row_mean
    row_var = jnp.mean(centred * centred, axis=-1, keepdims=True)
    return centred * lax.rsqrt(row_var + norm_eps) * norm_gain


def pair_slots(pair_ids, experts):
    flat_ids = pair_ids.reshape(-1)
    onehot = (flat_ids[:, None] == jnp.arange(experts, dtype=jnp.int32)[None, :]).astype(jnp.int32)
    before = jnp.cumsum(onehot, axis=0) - onehot
    return jnp.sum(before * onehot, axis=1).reshape(pair_ids.shape)


def shards(
    mixer_in,
    doc_ids,
    mix_scale,
    out_proj,
    residual,
    mix_gain,
    expert_ids,
    expert_weight,
    w_gate,
    w_up,
    w_down,
    out_gain,
):
    tok_rows, chan_cols = mixer_in.shape
    features = mix_gain.shape[0]
    tail_rows = (mixer_in[tok_rows - pool_reach :], doc_ids[tok_rows - pool_reach :])
    before_vals, before_doc = passed_along((tail_rows[0], tail_rows[1]), "sp", 1)
    extended = jnp.concatenate([before_vals, mixer_in], axis=0).astype(jnp.float32)
    extended_doc = jnp.concatenate([before_doc, doc_ids], axis=0)
    positions = lax.axis_index("sp") * tok_rows + jnp.arange(tok_rows, dtype=jnp.int32)
    channel = lax.axis_index("tp") * chan_cols + jnp.arange(chan_cols, dtype=jnp.int32)
    window = jnp.left_shift(jnp.int32(2), channel // (features // 4))
    window_sum = jnp.zeros((tok_rows, chan_cols), jnp.float32)
    window_count = jnp.zeros((tok_rows, chan_cols), jnp.float32)
    for lag_step in range(pool_reach + 1):
        shifted = extended[pool_reach - lag_step : pool_reach - lag_step + tok_rows]
        same_doc = (
            extended_doc[pool_reach - lag_step : pool_reach - lag_step + tok_rows] == doc_ids
        ) & (positions >= lag_step)
        in_window = (same_doc[:, None] & (lag_step < window)[None, :]).astype(jnp.float32)
        window_sum = window_sum + in_window * shifted
        window_count = window_count + in_window
    mixed_rows = ((window_sum / window_count - extended[pool_reach:]) * mix_scale).astype(
        jnp.bfloat16
    )
    share_rows = tok_rows // lax.axis_size("tp")
    projected = lax.psum_scatter(
        jnp.dot(mixed_rows, out_proj, preferred_element_type=jnp.float32).astype(jnp.bfloat16),
        "tp",
        scatter_dimension=0,
        tiled=True,
    ).astype(jnp.float32)
    own_residual = lax.dynamic_slice_in_dim(
        residual, lax.axis_index("tp") * share_rows, share_rows, 0
    )
    normed_share = layer_norm(
        alpha_res * own_residual.astype(jnp.float32) + projected, mix_gain
    ).astype(jnp.bfloat16)
    normed = lax.all_gather(normed_share, "tp", axis=0, tiled=True)
    experts = lax.axis_size("sp")
    capacity = 4 * tok_rows // experts
    ranks = pair_slots(expert_ids, experts)
    target = expert_ids * capacity + ranks
    slot_ids = jnp.arange(experts * capacity, dtype=jnp.int32)[:, None]
    select = ((target[None, :, 0] == slot_ids) | (target[None, :, 1] == slot_ids)).astype(
        jnp.bfloat16
    )
    source_rows = lax.dynamic_slice_in_dim(normed, lax.axis_index("tp") * chan_cols, chan_cols, 1)
    outgoing = jnp.dot(select, source_rows, preferred_element_type=jnp.float32).astype(jnp.bfloat16)
    outgoing = outgoing.reshape(experts, capacity, source_rows.shape[1])
    incoming = lax.all_to_all(outgoing, "sp", split_axis=0, concat_axis=0, tiled=True)
    incoming = lax.all_gather(incoming, "tp", axis=2, tiled=True)
    senders, slot_count, width_all = incoming.shape
    flat_in = incoming.reshape(senders * slot_count, width_all)
    gate_pre = jnp.dot(flat_in, w_gate[0], preferred_element_type=jnp.float32)
    upper = jnp.dot(flat_in, w_up[0], preferred_element_type=jnp.float32)
    hidden = (jax.nn.silu(gate_pre) * upper).astype(jnp.bfloat16)
    partial_value = jnp.dot(hidden, w_down[0], preferred_element_type=jnp.float32).astype(
        jnp.bfloat16
    )
    returned = lax.all_to_all(
        partial_value.reshape(senders, slot_count, width_all),
        "sp",
        split_axis=0,
        concat_axis=0,
        tiled=True,
    )
    picked = returned.reshape(experts * capacity, features)[target]
    weighted = jnp.sum(picked.astype(jnp.float32) * expert_weight[:, :, None], axis=1)
    routed = lax.psum(weighted.astype(jnp.bfloat16), "tp").astype(jnp.float32)
    return layer_norm(alpha_res * normed.astype(jnp.float32) + routed, out_gain).astype(
        jnp.bfloat16
    )


def solution(mesh):
    placed = (
        P("sp", "tp"),
        P("sp"),
        P("tp"),
        P("tp", None),
        P("sp", None),
        P(),
        P("sp", None),
        P("sp", None),
        P("sp", None, "tp"),
        P("sp", None, "tp"),
        P("sp", "tp", None),
        P(),
    )
    return jax.shard_map(
        shards, mesh=mesh, in_specs=placed, out_specs=P("sp", None), check_vma=False
    )
```

profile of v0, /device:TPU:0, one launch (start us, length us, event | category | flops | bytes accessed | tf_op | source)
XLA Modules:
  0.0 340.1 jit_solution(10196914106169270172)
XLA Ops:
  6.5 0.0 copy-start
  6.5 0.0 reduce-scatter.2.cloned.1.call-start
  6.5 0.9 slice.114
  7.4 4.9 %collective-permute-start.1 = (s32[15]{0:T(128)S(1)}, s32[15]{0:T(128)S(1)}, u32[]{:S(2)}, u32[]{:S(2)}) collective-permute-start(s32[15]{0:T(128)S(1)} %slice.114), channel_id=1, source_target_pairs={{0,4},{4,8},{8,12},{12,16},{16,20},{20,24},{24,28},{1,5},{5,9},{9,... | collective-permute-start | bytes 188 | tf_op jit(solution)/shard_map/ppermute | solution.py:14
  12.3 0.7 slice.112
  13.0 3.4 %collective-permute-start = (bf16[15,512]{1,0:T(8,128)(2,1)S(1)}, bf16[15,512]{1,0:T(8,128)(2,1)S(1)}, u32[]{:S(2)}, u32[]{:S(2)}) collective-permute-start(bf16[15,512]{1,0:T(8,128)(2,1)S(1)} %slice.112), channel_id=1, source_target_pairs={{0,4},{4,8},{8,12},{12,16},{16,20},{20,24},{24,28},{1,5},{5,9},{9,... | collective-permute-start | bytes 46088 | tf_op jit(solution)/shard_map/ppermute | solution.py:14
  16.7 0.0 collective-permute-done.1
  16.7 0.8 pad_add_fusion
  17.4 0.8 compare_and_fusion.14
  18.2 0.0 collective-permute-done
  18.2 1.0 maximum_convert_fusion
  19.2 0.0 copy-done
  19.2 0.0 copy-start.3
  19.3 0.0 copy-start.4
  19.3 0.0 copy-start.6
  19.3 5.9 %convolution_convert_fusion = bf16[256,2048]{1,0:T(8,128)(2,1)} fusion(bf16[512,2048]{1,0:T(8,128)(2,1)S(1)} %copy-done, f32[271,512]{1,0:T(8,128)S(1)} %maximum_convert_fusion, f32[512]{0:T(512)} %param.14, pred[512]{0:T(512)(128)(4,1)S(1)} %get-tuple-element.24, pred[512]{0:T(512)(128)(4,1)S(1)} %get-tuple-element.25, ...), kind=kOutput, calls=%fused_computation.11 | convolution fusion | flops 548143104 | bytes 11552768 | tf_op jit(solution)/shard_map/dot_general | solution.py:69
  25.2 0.0 reduce-scatter.2.cloned.1.call-update
  25.2 0.0 all-gather.3.cloned.1.call-start
  25.3 26.5 %reduce-scatter.2.cloned.1.call-done = bf16[64,2048]{1,0:T(8,128)(2,1)} async-done(((bf16[256,2048]{1,0:T(8,128)(2,1)}), bf16[64,2048]{1,0:T(8,128)(2,1)}) %reduce-scatter.2.cloned.1.call-update) | async-done | bytes 262160 | tf_op jit(solution)/shard_map/reduce_scatter | solution.py:68
  51.8 0.0 copy-done.3
  51.8 1.1 fusion.53
  53.0 1.2 multiply_reduce_fusion.2
  54.2 0.0 copy-done.4
  54.2 1.8 multiply_convert_fusion.2
  56.0 0.0 all-gather.3.cloned.1.call-update
  56.0 0.0 all-gather.5.cloned.1.call-start
  56.0 0.0 copy-done.6
  56.1 0.1 copy.24
  56.2 0.1 eq.119
  56.3 0.1 eq.115
  56.5 1.1 reduce-window.6
  57.6 0.2 slice_reduce_fusion
  57.9 0.1 fusion.56
  58.0 0.1 reshape.149
  58.2 0.1 copy.26
  58.2 14.7 %all-gather.3.cloned.1.call-done = bf16[256,2048]{1,0:T(8,128)(2,1)} async-done(((bf16[64,2048]{1,0:T(8,128)(2,1)}), bf16[256,2048]{1,0:T(8,128)(2,1)}) %all-gather.3.cloned.1.call-update) | async-done | bytes 1048592 | tf_op jit(solution)/shard_map/all_gather | solution.py:80
  72.9 1.4 convolution_convert_fusion.1
  74.3 31.5 %all_to_all.10 = bf16[8,128,512]{2,1,0:T(8,128)(2,1)} all-to-all(bf16[8,128,512]{2,1,0:T(8,128)(2,1)S(1)} %bitcast.35), channel_id=1, replica_groups=mesh['sp'=8,'tp'=4] {'sp'}, dimensions={0} | all-to-all | bytes 2097152 | tf_op jit(solution)/shard_map/all_to_all | solution.py:92
  105.8 0.0 all-gather.5.cloned.1.call-update
  105.9 32.7 %all-gather.5.cloned.1.call-done = bf16[8,128,2048]{2,1,0:T(8,128)(2,1)} async-done(((bf16[8,128,512]{2,1,0:T(8,128)(2,1)}), bf16[8,128,2048]{2,1,0:T(8,128)(2,1)}) %all-gather.5.cloned.1.call-update) | async-done | bytes 4194320 | tf_op jit(solution)/shard_map/all_gather | solution.py:93
  138.6 11.7 %fusion.4 = f32[1024,1408]{1,0:T(8,128)} fusion(bf16[1024,2048]{1,0:T(8,128)(2,1)} %bitcast.38, bf16[1,2048,1408]{2,1,0:T(8,128)(2,1)} %param.20), kind=kOutput, calls=%fused_computation.5 | convolution fusion | flops 5905580032 | bytes 15728640 | tf_op jit(solution)/shard_map/dot_general | solution.py:96
  150.3 20.6 %fusion.10 = bf16[1024,2048]{1,0:T(8,128)(2,1)} fusion(bf16[1,1408,2048]{2,1,0:T(8,128)(2,1)} %param.22, f32[1024,1408]{1,0:T(8,128)} %fusion.4, bf16[1024,2048]{1,0:T(8,128)(2,1)} %bitcast.39, bf16[1,2048,1408]{2,1,0:T(8,128)(2,1)} %param.21), kind=kOutput, calls=%fused_computation.9 | convolution fusion | flops 11821907968 | bytes 25690112 | tf_op jit(solution)/shard_map/dot_general | solution.py:99
  171.0 0.0 copy-start.7
  171.0 5.6 %all-to-all-start.1 = ((bf16[8,128,2048]{2,1,0:T(8,128)(2,1)}), bf16[8,128,2048]{2,1,0:T(8,128)(2,1)}, u32[]{:S(2)}, u32[]{:S(2)}) async-start(bf16[8,128,2048]{2,1,0:T(8,128)(2,1)} %bitcast.34), calls=%async_computation.2 | async-start | bytes 8388608 | tf_op jit(solution)/shard_map/all_to_all | solution.py:102
  176.6 0.0 all-reduce.2.cloned.1.call-start
  176.7 0.1 copy.27
  176.8 0.1 reshape.156
  177.0 0.0 copy-done.7
  177.0 0.1 copy.28
  177.1 93.2 %all-to-all-done.1 = bf16[8,128,2048]{2,1,0:T(8,128)(2,1)} async-done(((bf16[8,128,2048]{2,1,0:T(8,128)(2,1)}), bf16[8,128,2048]{2,1,0:T(8,128)(2,1)}, u32[]{:S(2)}, u32[]{:S(2)}) %all-to-all-start.1) | async-done | bytes 4194336 | tf_op jit(solution)/shard_map/all_to_all | solution.py:102
  270.3 8.2 %gather_fusion = bf16[512,2048]{1,0:T(8,128)(2,1)} fusion(bf16[1024,2048]{1,0:T(8,128)(2,1)} %bitcast.10, s32[1024]{0:T(1024)S(1)} %pad_clamp_fusion), kind=kCustom, calls=%fused_computation | custom fusion | bytes 4196352 | tf_op jit(solution)/shard_map/gather | solution.py:109
  278.5 5.4 %reshape.164 = f32[256,2,2048]{2,1,0:T(2,128)} reshape(bf16[512,2048]{1,0:T(8,128)(2,1)} %gather_fusion) | data formatting | bytes 6291456 | tf_op jit(solution)/shard_map/convert_element_type | solution.py:110
  283.9 0.0 copy-start.1
  283.9 0.0 copy-start.5
  283.9 9.9 %multiply_reduce_fusion = bf16[256,2048]{1,0:T(8,128)(2,1)} fusion(f32[256,2,2048]{2,1,0:T(2,128)} %reshape.164, f32[256,2]{1,0:T(8,128)S(1)} %copy.28), kind=kLoop, calls=%fused_computation.8 | loop fusion | flops 1572864 | bytes 5244928 | tf_op jit(solution)/shard_map/reduce_sum | solution.py:110
  293.9 0.0 all-reduce.2.cloned.1.call-update
  293.9 34.6 %all-reduce.2.cloned.1.call-done = bf16[256,2048]{1,0:T(8,128)(2,1)} async-done(((bf16[256,2048]{1,0:T(8,128)(2,1)}), bf16[256,2048]{1,0:T(8,128)(2,1)}) %all-reduce.2.cloned.1.call-update) | async-done | bytes 1048592 | tf_op jit(solution)/shard_map/psum | solution.py:111
  328.4 0.0 copy-done.1
  328.4 0.0 copy-start.2
  328.5 1.7 fusion.16
  330.2 1.8 multiply_reduce_fusion.1
  332.0 0.0 copy-done.5
  332.0 0.0 copy-done.2
  332.0 1.5 multiply_convert_fusion.1
  (18 shorter events, 0.2 us)
Async XLA Ops:
  6.5 12.7 %copy-start = (bf16[512,2048]{1,0:T(8,128)(2,1)S(1)}, bf16[512,2048]{1,0:T(8,128)(2,1)}, u32[]{:S(2)}) copy-start(bf16[512,2048]{1,0:T(8,128)(2,1)} %param.15) | copy-start | bytes 6291460
  6.5 45.3 %reduce-scatter.2.cloned.1.call-start = ((), (), s32[]{:S(2)}) async-start(), calls=%async_computation.3 | async-start | bytes 1310720 | tf_op jit(solution)/shard_map/reduce_scatter | solution.py:68
  7.4 9.2 %collective-permute-start.1 = (s32[15]{0:T(128)S(1)}, s32[15]{0:T(128)S(1)}, u32[]{:S(2)}, u32[]{:S(2)}) collective-permute-start(s32[15]{0:T(128)S(1)} %slice.114), channel_id=1, source_target_pairs={{0,4},{4,8},{8,12},{12,16},{16,20},{20,24},{24,28},{1,5},{5,9},{9,... | collective-permute-start | bytes 188 | tf_op jit(solution)/shard_map/ppermute | solution.py:14
  13.0 5.2 %collective-permute-start = (bf16[15,512]{1,0:T(8,128)(2,1)S(1)}, bf16[15,512]{1,0:T(8,128)(2,1)S(1)}, u32[]{:S(2)}, u32[]{:S(2)}) collective-permute-start(bf16[15,512]{1,0:T(8,128)(2,1)S(1)} %slice.112), channel_id=1, source_target_pairs={{0,4},{4,8},{8,12},{12,16},{16,20},{20,24},{24,28},{1,5},{5,9},{9,... | collective-permute-start | bytes 46088 | tf_op jit(solution)/shard_map/ppermute | solution.py:14
  19.2 32.6 %copy-start.3 = (bf16[256,2048]{1,0:T(8,128)(2,1)S(1)}, bf16[256,2048]{1,0:T(8,128)(2,1)}, u32[]{:S(2)}) copy-start(bf16[256,2048]{1,0:T(8,128)(2,1)} %param.16) | copy-start | bytes 3145732
  19.3 34.9 %copy-start.4 = (f32[2048]{0:T(1024)S(1)}, f32[2048]{0:T(1024)}, u32[]{:S(2)}) copy-start(f32[2048]{0:T(1024)} %param.17) | copy-start | bytes 24580
  19.3 36.8 %copy-start.6 = (s32[256,2]{0,1:T(2,128)S(1)}, s32[256,2]{0,1:T(2,128)}, u32[]{:S(2)}) copy-start(s32[256,2]{0,1:T(2,128)} %param.18) | copy-start | bytes 6148
  25.2 47.7 %all-gather.3.cloned.1.call-start = ((), (), s32[]{:S(2)}) async-start(), calls=%async_computation.4 | async-start | bytes 1310720 | tf_op jit(solution)/shard_map/all_gather | solution.py:80
  56.0 82.6 %all-gather.5.cloned.1.call-start = ((), (), s32[]{:S(2)}) async-start(), calls=%async_computation.5 | async-start | bytes 5242880 | tf_op jit(solution)/shard_map/all_gather | solution.py:93
  171.0 6.0 %copy-start.7 = (f32[256,2]{0,1:T(2,128)S(1)}, f32[256,2]{0,1:T(2,128)}, u32[]{:S(2)}) copy-start(f32[256,2]{0,1:T(2,128)} %param.19) | copy-start | bytes 6148
  171.0 99.3 %all-to-all-start.1 = ((bf16[8,128,2048]{2,1,0:T(8,128)(2,1)}), bf16[8,128,2048]{2,1,0:T(8,128)(2,1)}, u32[]{:S(2)}, u32[]{:S(2)}) async-start(bf16[8,128,2048]{2,1,0:T(8,128)(2,1)} %bitcast.34), calls=%async_computation.2 | async-start | bytes 8388608 | tf_op jit(solution)/shard_map/all_to_all | solution.py:102
  176.6 151.8 %all-reduce.2.cloned.1.call-start = ((), (), s32[]{:S(2)}) async-start(), calls=%async_computation.6 | async-start | bytes 2097152 | tf_op jit(solution)/shard_map/psum | solution.py:111
  283.9 44.5 %copy-start.1 = (bf16[256,2048]{1,0:T(8,128)(2,1)S(1)}, bf16[256,2048]{1,0:T(8,128)(2,1)}, u32[]{:S(2)}) copy-start(bf16[256,2048]{1,0:T(8,128)(2,1)} %all-gather.3.cloned.1.call-done) | copy-start | bytes 3145732
  283.9 48.1 %copy-start.5 = (f32[2048]{0:T(1024)S(1)}, f32[2048]{0:T(1024)}, u32[]{:S(2)}) copy-start(f32[2048]{0:T(1024)} %param.23) | copy-start | bytes 24580
  328.4 3.5 %copy-start.2 = (bf16[256,2048]{1,0:T(8,128)(2,1)S(1)}, bf16[256,2048]{1,0:T(8,128)(2,1)}, u32[]{:S(2)}) copy-start(bf16[256,2048]{1,0:T(8,128)(2,1)} %all-reduce.2.cloned.1.call-done) | copy-start | bytes 3145732
Sparse Core Ops, SparseCore 0:
  25.3 26.4 reduce-scatter.1
  56.1 16.7 all-gather.2
  106.0 32.5 all-gather.4
  294.0 34.4 all-reduce.1
where the time goes:
time: 341 us; the launch traced here: 340 us
  waiting for transfers between devices  202 us (59%)
  matrix products  39.7 us (12%)
  blocking collectives  31.5 us (9%)
  other arithmetic  23.1 us (7%)
  local copies, waits for them, and re-layouts  16.5 us (5%)
  starting transfers between devices  14.1 us (4%)
  between operations  13.4 us (4%)
    all_to_all x1, waiting for transfers between devices, shards(): lax.all_to_all(partial_value.reshape(senders, slot_count, width_all), 'sp...  93.2 us
    psum x1, waiting for transfers between devices, shards(): routed = lax.psum(weighted.astype(jnp.bfloat16), 'tp').astype(jnp.float32)  34.6 us
    all_gather x1, waiting for transfers between devices, shards(): incoming = lax.all_gather(incoming, 'tp', axis=2, tiled=True)  32.7 us
    all_to_all x1, blocking collectives, shards(): lax.all_to_all(outgoing, 'sp', split_axis=0, concat_axis=0, tiled=True)  31.5 us
    reduce_scatter x1, waiting for transfers between devices, shards(): lax.psum_scatter(jnp.dot(mixed_rows, out_proj, preferred_element_type=jnp...  26.5 us
    dot_general x1, matrix products, shards(): jnp.dot(hidden, w_down[0], preferred_element_type=jnp.float32)  20.6 us
    all_gather x1, waiting for transfers between devices, shards(): normed = lax.all_gather(normed_share, 'tp', axis=0, tiled=True)  14.7 us
    dot_general x1, matrix products, shards(): gate_pre = jnp.dot(flat_in, w_gate[0], preferred_element_type=jnp.float32)  11.7 us
  transfers between devices with their start and end apart: 7, of which 5 were waited for; matrix products, arithmetic and copies ran while one was open for 1% of the time, Pallas kernels for 0%

commit v1 on v0

v1 whole, which is shorter than its diff:
```python
import functools

import jax
import jax.numpy as jnp
from jax import lax
from jax.experimental import pallas as pl
from jax.experimental.pallas import tpu as pltpu
from jax.sharding import PartitionSpec as P

MESH = pl.DeviceIdType.MESH
DMA = pltpu.SemaphoreType.DMA
f32 = jnp.float32
bf16 = jnp.bfloat16

alpha_res = 1.4142135623730951
norm_eps = 1e-05
pool_reach = 15


def passed_along(value, axis, steps):
    count = lax.axis_size(axis)
    initial, last = (max(0, -steps), min(count, count - steps))
    return lax.ppermute(value, axis, [(source, source + steps) for source in range(initial, last)])


def layer_norm(summed, norm_gain):
    row_mean = jnp.mean(summed, axis=-1, keepdims=True)
    centred = summed - row_mean
    row_var = jnp.mean(centred * centred, axis=-1, keepdims=True)
    return centred * lax.rsqrt(row_var + norm_eps) * norm_gain


def pair_slots(pair_ids, experts):
    flat_ids = pair_ids.reshape(-1)
    onehot = (flat_ids[:, None] == jnp.arange(experts, dtype=jnp.int32)[None, :]).astype(jnp.int32)
    before = jnp.cumsum(onehot, axis=0) - onehot
    return jnp.sum(before * onehot, axis=1).reshape(pair_ids.shape)


def wrapped(value, count):
    return lax.rem(value + 2 * count, count)


def place(n_tp):
    me = lax.axis_index("tp")
    return lax.div(me, 2), lax.rem(me, 2)


def sent(src, dst, send_sem, recv_sem, device):
    return pltpu.make_async_remote_copy(
        src_ref=src,
        dst_ref=dst,
        send_sem=send_sem,
        recv_sem=recv_sem,
        device_id=device,
        device_id_type=MESH,
    )


def greet(n_sp, n_tp):
    y, core = place(n_tp)
    n_y = n_tp // 2
    barrier = pltpu.get_barrier_semaphore()
    pl.semaphore_signal(
        barrier, inc=1, device_id={"tp": y * 2 + 1 - core}, device_id_type=MESH
    )
    for j in range(1, n_y):
        pl.semaphore_signal(
            barrier, inc=1, device_id={"tp": wrapped(y + j, n_y) * 2 + core}, device_id_type=MESH
        )
    if n_sp > 1:
        me = lax.axis_index("sp")

        def tell(k, carry):
            pl.semaphore_signal(
                barrier, inc=1, device_id={"sp": wrapped(me + k, n_sp)}, device_id_type=MESH
            )
            return carry

        lax.fori_loop(1, n_sp, tell, 0)
    pl.semaphore_wait(barrier, n_y + n_sp - 1)


def spread(n_y, y, core, part, sems):
    send_y, recv_y, send_c, recv_c = sems
    other = {"tp": y * 2 + 1 - core}
    own = part(y, core)
    along = []
    for j in range(1, n_y):
        copy = sent(
            own, own, send_y.at[j], recv_y.at[j], {"tp": wrapped(y + j, n_y) * 2 + core}
        )
        copy.start()
        along.append(copy)
    across = [sent(own, own, send_c.at[0], recv_c.at[0], other)]
    across[0].start()
    for j in range(1, n_y):
        came = part(wrapped(y - j, n_y), core)
        sent(came, came, send_y.at[j], recv_y.at[j], other).wait_recv()
        copy = sent(came, came, send_c.at[j], recv_c.at[j], other)
        copy.start()
        across.append(copy)
    for j in range(n_y):
        came = part(wrapped(y - j, n_y), 1 - core)
        sent(came, came, send_c.at[j], recv_c.at[j], other).wait_recv()
    for copy in along + across:
        copy.wait_send()


def project_kernel(
    n_tp, proj, residual, gain, normed, recv_a, send_b, recv_b, sa, ra, sb, rb, sy, ry, sc, rc
):
    y, core = place(n_tp)
    n_y = n_tp // 2
    share = proj.shape[0] // n_tp
    other = {"tp": y * 2 + 1 - core}

    def rows(y_of, core_of):
        return pl.ds(pl.multiple_of((core_of * n_y + y_of) * share, share), share)

    greet(1, n_tp)
    halves = {}
    for j in list(range(1, n_y)) + [0]:
        y_to = wrapped(y + j, n_y)
        halves[j] = sent(
            proj.at[rows(y_to, 1 - core)], recv_a.at[j], sa.at[j], ra.at[j], other
        )
        halves[j].start()
    along = []
    for j in range(1, n_y):
        y_to = wrapped(y + j, n_y)
        halves[j].wait_recv()
        send_b[j] = (proj[rows(y_to, core), :].astype(f32) + recv_a[j].astype(f32)).astype(bf16)
        copy = sent(
            send_b.at[j], recv_b.at[j], sb.at[j], rb.at[j], {"tp": y_to * 2 + core}
        )
        copy.start()
        along.append(copy)
    halves[0].wait_recv()
    summed = proj[rows(y, core), :].astype(f32) + recv_a[0].astype(f32)
    summed = summed + alpha_res * residual[rows(y, core), :].astype(f32)
    for j in range(1, n_y):
        along[j - 1].wait_recv()
        summed = summed + recv_b[j].astype(f32)
    normed[rows(y, core), :] = layer_norm(summed, gain[...]).astype(bf16)
    spread(n_y, y, core, lambda a, b: normed.at[rows(a, b)], (sy, ry, sc, rc))
    for copy in list(halves.values()) + along:
        copy.wait_send()


def dispatch_kernel(
    n_sp, n_tp, select, normed, x, send, s1, r1, s2, r2, s3, r3
):
    y, core = place(n_tp)
    n_y = n_tp // 2
    me = lax.axis_index("sp")
    cap = select.shape[0] // n_sp
    width = normed.shape[1] // n_tp
    other = {"tp": y * 2 + 1 - core}

    def cols(y_of, core_of):
        return pl.ds(pl.multiple_of((core_of * n_y + y_of) * width, width), width)

    def rows(block):
        return pl.ds(pl.multiple_of(block * cap, cap), cap)

    own = cols(y, core)
    greet(n_sp, n_tp)

    def picked(block):
        return jnp.dot(
            select[rows(block), :], normed[:, own], preferred_element_type=f32
        ).astype(bf16)

    def first(k):
        to = wrapped(me + k, n_sp)
        return sent(send.at[rows(to)], x.at[rows(me), own], s1.at[k], r1.at[k], {"sp": to})

    def along(k, j):
        piece = x.at[rows(wrapped(me - k, n_sp)), own]
        return sent(piece, piece, s2.at[j, k], r2.at[j, k], {"tp": wrapped(y + j, n_y) * 2 + core})

    def across(k, j, core_of):
        piece = x.at[rows(wrapped(me - k, n_sp)), cols(wrapped(y - j, n_y), core_of)]
        return sent(piece, piece, s3.at[j, k], r3.at[j, k], other)

    def start_first(k, carry):
        to = wrapped(me + k, n_sp)
        send[rows(to), :] = picked(to)
        first(k).start()
        return carry

    lax.fori_loop(1, n_sp, start_first, 0)
    x[rows(me), own] = picked(me)

    def forward(k):
        for j in range(1, n_y):
            along(k, j).start()
        across(k, 0, core).start()

    def second(k):
        for j in range(1, n_y):
            came = x.at[rows(wrapped(me - k, n_sp)), cols(wrapped(y - j, n_y), core)]
            sent(came, came, s2.at[j, k], r2.at[j, k], other).wait_recv()
            across(k, j, core).start()

    forward(0)

    def body(k, carry):
        came = x.at[rows(wrapped(me - k, n_sp)), own]
        sent(came, came, s1.at[k], r1.at[k], other).wait_recv()
        forward(k)
        second(k - 1)
        return carry

    lax.fori_loop(1, n_sp, body, 0)
    second(n_sp - 1)

    def finish(k, carry):
        for j in range(n_y):
            across(k, j, 1 - core).wait_recv()
            across(k, j, core).wait_send()
        for j in range(1, n_y):
            along(k, j).wait_send()
        return carry

    lax.fori_loop(0, n_sp, finish, 0)

    def finish_first(k, carry):
        first(k).wait_send()
        return carry

    lax.fori_loop(1, n_sp, finish_first, 0)


def combine_kernel(
    n_sp, n_tp, partial, mix_hi, mix_lo, normed, gain, out,
    recv_a, send_b, recv_b, send_c, recv_c, routed,
    sa, ra, sb, rb, s1, r1, sy, ry, sc, rc,
):
    y, core = place(n_tp)
    n_y = n_tp // 2
    me = lax.axis_index("sp")
    cap = partial.shape[0] // n_sp
    features = partial.shape[1]
    width, half = features // n_tp, features // 2
    other = {"tp": y * 2 + 1 - core}

    def cols(y_of, core_of):
        return pl.ds(pl.multiple_of((core_of * n_y + y_of) * width, width), width)

    def sub(y_of):
        return pl.ds(pl.multiple_of(y_of * width, width), width)

    def rows(block):
        return pl.ds(pl.multiple_of(block * cap, cap), cap)

    def block_of(k):
        return wrapped(me + k + 1, n_sp)

    greet(n_sp, n_tp)

    def across(k):
        at = rows(block_of(k))
        far = pl.ds(pl.multiple_of((1 - core) * half, half), half)
        return sent(partial.at[at, far], recv_a.at[at], sa.at[k], ra.at[k], other)

    def along(k, j):
        at = rows(block_of(k))
        return sent(
            send_b.at[j, at], recv_b.at[j, at], sb.at[j, k], rb.at[j, k],
            {"tp": wrapped(y + j, n_y) * 2 + core},
        )

    def home(k):
        to = block_of(k)
        return sent(send_c.at[rows(to)], recv_c.at[rows(me)], s1.at[k], r1.at[k], {"sp": to})

    def start_a(k, carry):
        across(k).start()
        return carry

    lax.fori_loop(0, n_sp, start_a, 0)

    def start_b(k, carry):
        across(k).wait_recv()
        at = rows(block_of(k))
        for j in range(1, n_y):
            y_to = wrapped(y + j, n_y)
            send_b[j, at, :] = (
                partial[at, cols(y_to, core)].astype(f32) + recv_a[at, sub(y_to)].astype(f32)
            ).astype(bf16)
            along(k, j).start()
        return carry

    lax.fori_loop(0, n_sp, start_b, 0)

    def total(k):
        at = rows(block_of(k))
        summed = partial[at, cols(y, core)].astype(f32) + recv_a[at, sub(y)].astype(f32)
        for j in range(1, n_y):
            along(k, j).wait_recv()
            summed = summed + recv_b[j, at, :].astype(f32)
        return summed.astype(bf16)

    def start_c(k, carry):
        summed = total(k)
        send_c[rows(block_of(k)), :] = summed
        home(k).start()
        return carry

    lax.fori_loop(0, n_sp - 1, start_c, 0)
    recv_c[rows(me), :] = total(n_sp - 1)

    def finish_c(k, carry):
        came = recv_c.at[rows(wrapped(me - k - 1, n_sp))]
        sent(came, came, s1.at[k], r1.at[k], other).wait_recv()
        home(k).wait_send()
        return carry

    lax.fori_loop(0, n_sp - 1, finish_c, 0)
    routed[:, cols(y, core)] = (
        jnp.dot(mix_hi[...], recv_c[...], preferred_element_type=f32)
        + jnp.dot(mix_lo[...], recv_c[...], preferred_element_type=f32)
    ).astype(bf16)
    spread(n_y, y, core, lambda a, b: routed.at[:, cols(a, b)], (sy, ry, sc, rc))
    step = 64

    def norm(i, carry):
        at = pl.ds(pl.multiple_of(i * step, step), step)
        summed = alpha_res * normed[at, :].astype(f32) + routed[at, :].astype(f32)
        out[at, :] = layer_norm(summed, gain[...]).astype(bf16)
        return carry

    lax.fori_loop(0, out.shape[0] // step, norm, 0)

    def finish(k, carry):
        across(k).wait_send()
        for j in range(1, n_y):
            along(k, j).wait_send()
        return carry

    lax.fori_loop(0, n_sp, finish, 0)


def called(kernel, args, shape, scratch, number):
    return pl.pallas_call(
        kernel,
        out_shape=jax.ShapeDtypeStruct(shape, bf16),
        in_specs=[pl.BlockSpec(memory_space=pltpu.VMEM)] * len(args),
        out_specs=pl.BlockSpec(memory_space=pltpu.VMEM),
        scratch_shapes=scratch,
        compiler_params=pltpu.CompilerParams(
            collective_id=number, has_side_effects=True, vmem_limit_bytes=60 * 1024 * 1024
        ),
    )(*args)


def spread_sems(n_y):
    return [DMA((n_y,))] * 4


def project(proj, residual, gain, n_tp):
    rows, features = proj.shape
    n_y, share = n_tp // 2, rows // n_tp
    piece = pltpu.VMEM((n_y, share, features), bf16)
    return called(
        functools.partial(project_kernel, n_tp),
        (proj, residual, gain.reshape(1, features)),
        (rows, features),
        [piece] * 3 + [DMA((n_y,))] * 4 + spread_sems(n_y),
        0,
    )


def dispatch(select, normed, n_sp, n_tp):
    slots, features = select.shape[0], normed.shape[1]
    n_y = n_tp // 2
    return called(
        functools.partial(dispatch_kernel, n_sp, n_tp),
        (select, normed),
        (slots, features),
        [pltpu.VMEM((slots, features // n_tp), bf16)]
        + [DMA((n_sp,))] * 2
        + [DMA((n_y, n_sp))] * 4,
        1,
    )


def combine(partial, mix_hi, mix_lo, normed, gain, n_sp, n_tp):
    slots, features = partial.shape
    rows = normed.shape[0]
    n_y, width = n_tp // 2, features // n_tp
    return called(
        functools.partial(combine_kernel, n_sp, n_tp),
        (partial, mix_hi, mix_lo, normed, gain.reshape(1, features)),
        (rows, features),
        [
            pltpu.VMEM((slots, features // 2), bf16),
            pltpu.VMEM((n_y, slots, width), bf16),
            pltpu.VMEM((n_y, slots, width), bf16),
            pltpu.VMEM((slots, width), bf16),
            pltpu.VMEM((slots, width), bf16),
            pltpu.VMEM((rows, features), bf16),
        ]
        + [DMA((n_sp,))] * 2
        + [DMA((n_y, n_sp))] * 2
        + [DMA((n_sp,))] * 2
        + spread_sems(n_y),
        2,
    )


def shards(
    mixer_in,
    doc_ids,
    mix_scale,
    out_proj,
    residual,
    mix_gain,
    expert_ids,
    expert_weight,
    w_gate,
    w_up,
    w_down,
    out_gain,
):
    tok_rows, chan_cols = mixer_in.shape
    features = mix_gain.shape[0]
    tail_rows = (mixer_in[tok_rows - pool_reach :], doc_ids[tok_rows - pool_reach :])
    before_vals, before_doc = passed_along((tail_rows[0], tail_rows[1]), "sp", 1)
    extended = jnp.concatenate([before_vals, mixer_in], axis=0).astype(jnp.float32)
    extended_doc = jnp.concatenate([before_doc, doc_ids], axis=0)
    positions = lax.axis_index("sp") * tok_rows + jnp.arange(tok_rows, dtype=jnp.int32)
    channel = lax.axis_index("tp") * chan_cols + jnp.arange(chan_cols, dtype=jnp.int32)
    window = jnp.left_shift(jnp.int32(2), channel // (features // 4))
    window_sum = jnp.zeros((tok_rows, chan_cols), jnp.float32)
    window_count = jnp.zeros((tok_rows, chan_cols), jnp.float32)
    for lag_step in range(pool_reach + 1):
        shifted = extended[pool_reach - lag_step : pool_reach - lag_step + tok_rows]
        same_doc = (
            extended_doc[pool_reach - lag_step : pool_reach - lag_step + tok_rows] == doc_ids
        ) & (positions >= lag_step)
        in_window = (same_doc[:, None] & (lag_step < window)[None, :]).astype(jnp.float32)
        window_sum = window_sum + in_window * shifted
        window_count = window_count + in_window
    mixed_rows = ((window_sum / window_count - extended[pool_reach:]) * mix_scale).astype(
        jnp.bfloat16
    )
    n_sp, n_tp = lax.axis_size("sp"), lax.axis_size("tp")
    product = jnp.dot(mixed_rows, out_proj, preferred_element_type=f32).astype(bf16)
    experts = n_sp
    capacity = 4 * tok_rows // experts
    ranks = pair_slots(expert_ids, experts)
    target = expert_ids * capacity + ranks
    slot_ids = jnp.arange(experts * capacity, dtype=jnp.int32)
    select = (
        (target[None, :, 0] == slot_ids[:, None]) | (target[None, :, 1] == slot_ids[:, None])
    ).astype(bf16)
    mix = jnp.sum(
        jnp.where(target[:, :, None] == slot_ids[None, None, :], expert_weight[:, :, None], 0.0),
        axis=1,
    )
    mix_hi = lax.reduce_precision(mix, 8, 7)
    mix_lo = (mix - mix_hi).astype(bf16)
    mix_hi = mix_hi.astype(bf16)
    normed = project(product, residual, mix_gain, n_tp)
    flat_in = dispatch(select, normed, n_sp, n_tp)
    gate_pre = jnp.dot(flat_in, w_gate[0], preferred_element_type=f32)
    upper = jnp.dot(flat_in, w_up[0], preferred_element_type=f32)
    hidden = (jax.nn.silu(gate_pre) * upper).astype(bf16)
    partial_value = jnp.dot(hidden, w_down[0], preferred_element_type=f32).astype(bf16)
    return combine(partial_value, mix_hi, mix_lo, normed, out_gain, n_sp, n_tp)


def solution(mesh):
    placed = (
        P("sp", "tp"),
        P("sp"),
        P("tp"),
        P("tp", None),
        P("sp", None),
        P(),
        P("sp", None),
        P("sp", None),
        P("sp", None, "tp"),
        P("sp", None, "tp"),
        P("sp", "tp", None),
        P(),
    )
    return jax.shard_map(
        shards, mesh=mesh, in_specs=placed, out_specs=P("sp", None), check_vma=False
    )
```

time: 341 us -> 176 us (0.52)
  waiting for transfers between devices: 202 us -> 0.01 us
  Pallas kernels: 0 us -> 115 us
  blocking collectives: 31.5 us -> 0 us
  other arithmetic: 23.1 us -> 7.91 us
  between operations: 13.4 us -> 0.16 us
  local copies, waits for them, and re-layouts: 16.5 us -> 5.48 us
  starting transfers between devices: 14.1 us -> 8.3 us
    pallas_call x0 -> x3, Pallas kernels: none -> 115 us  [called(): pl.pallas_call(kernel, out_shape=jax.ShapeDtypeStruct(shape, bf16), in_sp...]
    all_to_all x1 -> x0, waiting for transfers between devices: 93.2 us -> none  [shards(): lax.all_to_all(partial_value.reshape(senders, slot_count, width_all), 'sp...]
    all_gather x2 -> x0, waiting for transfers between devices: 47.4 us -> none  [the longest x1 32.7 us: shards(): incoming = lax.all_gather(incoming, 'tp', axis=2, tiled=True)]
    psum x1 -> x0, waiting for transfers between devices: 34.6 us -> none  [shards(): routed = lax.psum(weighted.astype(jnp.bfloat16), 'tp').astype(jnp.float32)]
    all_to_all x1 -> x0, blocking collectives: 31.5 us -> none  [shards(): lax.all_to_all(outgoing, 'sp', split_axis=0, concat_axis=0, tiled=True)]
    reduce_scatter x1 -> x0, waiting for transfers between devices: 26.5 us -> none  [shards(): lax.psum_scatter(jnp.dot(mixed_rows, out_proj, preferred_element_type=jnp...]
    reduce_sum x5 -> x1, other arithmetic: 15.8 us -> 1.06 us  [shards(): jnp.sum(jnp.where(target[:, :, None] == slot_ids[None, None, :], expert_w...]
    gather x1 -> x0, local copies, waits for them, and re-layouts: 8.16 us -> none  [shards(): picked = returned.reshape(experts * capacity, features)[target]]
  transfers between devices with their start and end apart: 7 -> 2, of which waited for: 5 -> 0; matrix products, arithmetic and copies ran while one was open for 1% -> 5% of each run, Pallas kernels for 0% -> 0%
where the time goes in v1:
time: 176 us; the launch traced here: 175 us
  Pallas kernels  115 us (65%)
  matrix products  38.2 us (22%)
  starting transfers between devices  8.3 us (5%)
  other arithmetic  7.91 us (4%)
  local copies, waits for them, and re-layouts  5.48 us (3%)
    pallas_call x3, Pallas kernels, called(): pl.pallas_call(kernel, out_shape=jax.ShapeDtypeStruct(shape, bf16), in_sp...  115 us
    dot_general x1, matrix products, shards(): jnp.dot(hidden, w_down[0], preferred_element_type=f32).astype(bf16)  20.6 us
    dot_general x1, matrix products, shards(): gate_pre = jnp.dot(flat_in, w_gate[0], preferred_element_type=f32)  11.7 us
    ppermute x2, starting transfers between devices, passed_along(): lax.ppermute(value, axis, [(source, source + steps) for source in range(i...  8.3 us
    dot_general x1, matrix products, shards(): jnp.dot(mixed_rows, out_proj, preferred_element_type=f32).astype(bf16)  5.85 us
  transfers between devices with their start and end apart: 2, of which 0 were waited for; matrix products, arithmetic and copies ran while one was open for 5% of the time, Pallas kernels for 0%

profile of v1, /device:TPU:0, one launch (start us, length us, event | category | flops | bytes accessed | tf_op | source)
XLA Modules:
  0.0 175.1 jit_solution(12814695282549650843)
XLA Ops:
  0.0 0.0 copy-start
  0.0 0.9 slice.118
  0.9 4.9 %collective-permute-start.1 = (s32[15]{0:T(128)S(1)}, s32[15]{0:T(128)S(1)}, u32[]{:S(2)}, u32[]{:S(2)}) collective-permute-start(s32[15]{0:T(128)S(1)} %slice.118), channel_id=1, source_target_pairs={{0,4},{4,8},{8,12},{12,16},{16,20},{20,24},{24,28},{1,5},{5,9},{9,... | collective-permute-start | bytes 188 | tf_op jit(solution)/shard_map/ppermute | solution.py:23
  5.8 0.7 slice.116
  6.5 3.4 %collective-permute-start = (bf16[15,512]{1,0:T(8,128)(2,1)S(1)}, bf16[15,512]{1,0:T(8,128)(2,1)S(1)}, u32[]{:S(2)}, u32[]{:S(2)}) collective-permute-start(bf16[15,512]{1,0:T(8,128)(2,1)S(1)} %slice.116), channel_id=1, source_target_pairs={{0,4},{4,8},{8,12},{12,16},{16,20},{20,24},{24,28},{1,5},{5,9},{9,... | collective-permute-start | bytes 46088 | tf_op jit(solution)/shard_map/ppermute | solution.py:23
  10.1 0.8 copy.30
  10.9 0.1 eq.117
  11.1 0.1 eq.113
  11.2 1.1 reduce-window.6
  12.4 0.2 slice_reduce_fusion
  12.6 0.1 fusion.52
  12.7 0.1 reshape.118
  12.9 0.1 copy.32
  13.0 0.7 multiply_add_fusion
  13.7 1.1 select_reduce_fusion
  14.7 1.2 fusion.16
  15.9 1.0 fusion.18.select
  16.9 0.0 collective-permute-done.1
  16.9 0.8 pad_add_fusion
  17.7 0.8 compare_and_fusion.14
  18.5 0.0 collective-permute-done
  18.5 1.0 maximum_convert_fusion
  19.5 0.0 copy-done
  19.5 5.8 %convolution_convert_fusion.proj = bf16[256,2048]{1,0:T(8,128)(2,1)} fusion(bf16[512,2048]{1,0:T(8,128)(2,1)S(1)} %copy-done, f32[271,512]{1,0:T(8,128)S(1)} %maximum_convert_fusion, f32[512]{0:T(512)} %param.14, pred[512]{0:T(512)(128)(4,1)S(1)} %get-tuple-element.24, pred[512]{0:T(512)(128)(4,1)S(1)} %get-tuple-element.25, ...), kind=kOutput, calls=%fused_computation.9 | convolution fusion | flops 548143104 | bytes 11552768 | tf_op jit(solution)/shard_map/dot_general | solution.py:451
  25.4 21.2 %shard_map.118.normed = bf16[256,2048]{1,0:T(8,128)(2,1)} custom-call(bf16[256,2048]{1,0:T(8,128)(2,1)} %convolution_convert_fusion.proj, bf16[256,2048]{1,0:T(8,128)(2,1)} %residual.1, f32[1,2048]{1,0:T(1,128)} %bitcast.32), custom_call_target="tpu_custom_call" | custom-call | tf_op jit(solution)/shard_map/pallas_call | solution.py:347
  46.5 40.8 %shard_map.119 = bf16[1024,2048]{1,0:T(8,128)(2,1)} custom-call(bf16[1024,256]{1,0:T(8,128)(2,1)} %fusion.18.select, bf16[256,2048]{1,0:T(8,128)(2,1)} %shard_map.118.normed), custom_call_target="tpu_custom_call" | custom-call | tf_op jit(solution)/shard_map/pallas_call | solution.py:347
  87.4 11.7 %fusion.4 = f32[1024,1408]{1,0:T(8,128)} fusion(bf16[1024,2048]{1,0:T(8,128)(2,1)} %shard_map.119, bf16[1,2048,1408]{2,1,0:T(8,128)(2,1)} %param.20), kind=kOutput, calls=%fused_computation.4 | convolution fusion | flops 5905580032 | bytes 15728640 | tf_op jit(solution)/shard_map/dot_general | solution.py:469
  99.1 20.6 %fusion.10.partial = bf16[1024,2048]{1,0:T(8,128)(2,1)} fusion(bf16[1,1408,2048]{2,1,0:T(8,128)(2,1)} %param.22, f32[1024,1408]{1,0:T(8,128)} %fusion.4, bf16[1024,2048]{1,0:T(8,128)(2,1)} %shard_map.119, bf16[1,2048,1408]{2,1,0:T(8,128)(2,1)} %param.21), kind=kOutput, calls=%fused_computation.7 | convolution fusion | flops 11821907968 | bytes 25690112 | tf_op jit(solution)/shard_map/dot_general | solution.py:472
  119.7 53.1 %shard_map.120 = bf16[256,2048]{1,0:T(8,128)(2,1)} custom-call(bf16[1024,2048]{1,0:T(8,128)(2,1)} %fusion.10.partial, bf16[256,1024]{1,0:T(8,128)(2,1)} %get-tuple-element.6.mix_hi, bf16[256,1024]{1,0:T(8,128)(2,1)} %get-tuple-element.5.mix_lo, bf16[256,2048]{1,0:T(8,128)(2,1)} %shard_map.118.normed, f32[1,2048]{1,0:T(1,128)} %bitcast.33), custom_call_target="tpu_custom_call" | custom-call | tf_op jit(solution)/shard_map/pallas_call | solution.py:347
  172.8 2.3 %copy.34 = bf16[256,2048]{1,0:T(8,128)(2,1)} copy(bf16[256,2048]{1,0:T(8,128)(2,1)} %shard_map.120) | data formatting | bytes 2097152
  (12 shorter events, 0.2 us)
Async XLA Ops:
  0.0 19.5 %copy-start = (bf16[512,2048]{1,0:T(8,128)(2,1)S(1)}, bf16[512,2048]{1,0:T(8,128)(2,1)}, u32[]{:S(2)}) copy-start(bf16[512,2048]{1,0:T(8,128)(2,1)} %param.15) | copy-start | bytes 6291460
  0.9 16.0 %collective-permute-start.1 = (s32[15]{0:T(128)S(1)}, s32[15]{0:T(128)S(1)}, u32[]{:S(2)}, u32[]{:S(2)}) collective-permute-start(s32[15]{0:T(128)S(1)} %slice.118), channel_id=1, source_target_pairs={{0,4},{4,8},{8,12},{12,16},{16,20},{20,24},{24,28},{1,5},{5,9},{9,... | collective-permute-start | bytes 188 | tf_op jit(solution)/shard_map/ppermute | solution.py:23
  6.5 12.0 %collective-permute-start = (bf16[15,512]{1,0:T(8,128)(2,1)S(1)}, bf16[15,512]{1,0:T(8,128)(2,1)S(1)}, u32[]{:S(2)}, u32[]{:S(2)}) collective-permute-start(bf16[15,512]{1,0:T(8,128)(2,1)S(1)} %slice.116), channel_id=1, source_target_pairs={{0,4},{4,8},{8,12},{12,16},{16,20},{20,24},{24,28},{1,5},{5,9},{9,... | collective-permute-start | bytes 46088 | tf_op jit(solution)/shard_map/ppermute | solution.py:23

commit v2 on v1

--- a/solution.py
+++ b/solution.py
@@ -148,178 +148,192 @@
         copy.wait_send()
 
 
-def dispatch_kernel(
-    n_sp, n_tp, select, normed, x, send, s1, r1, s2, r2, s3, r3
+def experts_kernel(
+    n_sp, n_tp, select, normed, w_gate, w_up, w_down, mix_hi, mix_lo, gain, out,
+    x, send, gate_v, up_v, down_v, partial, recv_a, send_b, recv_b, send_c, recv_c, routed,
+    sw, s1, r1, s2, r2, s3, r3, sa, ra, sb, rb, s4, r4, sy, ry, sc, rc,
 ):
     y, core = place(n_tp)
     n_y = n_tp // 2
     me = lax.axis_index("sp")
     cap = select.shape[0] // n_sp
-    width = normed.shape[1] // n_tp
+    features = normed.shape[1]
+    width, half = features // n_tp, features // 2
+    per = max(1, min(n_sp, 256 // cap))
+    chunks = n_sp // per
     other = {"tp": y * 2 + 1 - core}
+
+    def peer(k, sign):
+        outer = wrapped(lax.div(me, 2) + sign * lax.div(k, 2), n_sp // 2)
+        return outer * 2 + wrapped(lax.rem(me, 2) + sign * lax.rem(k, 2), 2)
 
     def cols(y_of, core_of):
         return pl.ds(pl.multiple_of((core_of * n_y + y_of) * width, width), width)
 
+    def sub(y_of):
+        return pl.ds(pl.multiple_of(y_of * width, width), width)
+
     def rows(block):
         return pl.ds(pl.multiple_of(block * cap, cap), cap)
 
+    def along_tp(j):
+        return {"tp": wrapped(y + j, n_y) * 2 + core}
+
     own = cols(y, core)
+    loads = [
+        pltpu.make_async_copy(source.at[0], held, sw.at[n])
+        for n, (source, held) in enumerate(((w_gate, gate_v), (w_up, up_v), (w_down, down_v)))
+    ]
+    for load in loads:
+        load.start()
     greet(n_sp, n_tp)
 
-    def picked(block):
-        return jnp.dot(
-            select[rows(block), :], normed[:, own], preferred_element_type=f32
+    def first(k):
+        to = peer(k, 1)
+        return sent(send.at[rows(k)], x.at[rows(k), own], s1.at[k], r1.at[k], {"sp": to})
+
+    def along(k, j):
+        piece = x.at[rows(k), own]
+        return sent(piece, piece, s2.at[j, k], r2.at[j, k], along_tp(j))
+
+    def across(k, j, core_of):
+        piece = x.at[rows(k), cols(wrapped(y - j, n_y), core_of)]
+        return sent(piece, piece, s3.at[j, k], r3.at[j, k], other)
+
+    def start_first(k, carry):
+        send[rows(k), :] = jnp.dot(
+            select[rows(peer(k, 1)), :], normed[:, own], preferred_element_type=f32
         ).astype(bf16)
-
-    def first(k):
-        to = wrapped(me + k, n_sp)
-        return sent(send.at[rows(to)], x.at[rows(me), own], s1.at[k], r1.at[k], {"sp": to})
-
-    def along(k, j):
-        piece = x.at[rows(wrapped(me - k, n_sp)), own]
-        return sent(piece, piece, s2.at[j, k], r2.at[j, k], {"tp": wrapped(y + j, n_y) * 2 + core})
-
-    def across(k, j, core_of):
-        piece = x.at[rows(wrapped(me - k, n_sp)), cols(wrapped(y - j, n_y), core_of)]
-        return sent(piece, piece, s3.at[j, k], r3.at[j, k], other)
-
-    def start_first(k, carry):
-        to = wrapped(me + k, n_sp)
-        send[rows(to), :] = picked(to)
         first(k).start()
         return carry
 
     lax.fori_loop(1, n_sp, start_first, 0)
-    x[rows(me), own] = picked(me)
-
-    def forward(k):
+    x[rows(0), :] = jnp.dot(
+        select[rows(me), :], normed[...], preferred_element_type=f32
+    ).astype(bf16)
+
+    def hop_one(i):
+        def body(k, carry):
+            first(k).wait_recv()
+            for j in range(1, n_y):
+                along(k, j).start()
+            across(k, 0, core).start()
+            return carry
+
+        lax.fori_loop(jnp.maximum(i * per, 1), i * per + per, body, 0)
+
+    def hop_two(i):
+        def body(k, carry):
+            for j in range(1, n_y):
+                came = x.at[rows(k), cols(wrapped(y - j, n_y), core)]
+                sent(came, came, s2.at[j, k], r2.at[j, k], other).wait_recv()
+                across(k, j, core).start()
+            return carry
+
+        lax.fori_loop(jnp.maximum(i * per, 1), i * per + per, body, 0)
+
+    def hop_three(i):
+        def body(k, carry):
+            for j in range(n_y):
+                across(k, j, 1 - core).wait_recv()
+            return carry
+
+        lax.fori_loop(jnp.maximum(i * per, 1), i * per + per, body, 0)
+
+    def compute(i):
+        at = pl.ds(pl.multiple_of(i * per * cap, per * cap), per * cap)
+        taken = x[at, :]
+        gate_pre = jnp.dot(taken, gate_v[...], preferred_element_type=f32)
+        upper = jnp.dot(taken, up_v[...], preferred_element_type=f32)
+        hidden = (gate_pre / (1.0 + jnp.exp(-gate_pre)) * upper).astype(bf16)
+        partial[at, :] = jnp.dot(hidden, down_v[...], preferred_element_type=f32).astype(bf16)
+
+    def side(k):
+        far = pl.ds(pl.multiple_of((1 - core) * half, half), half)
+        return sent(partial.at[rows(k), far], recv_a.at[rows(k)], sa.at[k], ra.at[k], other)
+
+    def lane(k, j):
+        return sent(
+            send_b.at[j, rows(k)], recv_b.at[j, rows(k)], sb.at[j, k], rb.at[j, k], along_tp(j)
+        )
+
+    def home(k):
+        return sent(
+            send_c.at[rows(k)], recv_c.at[rows(me)], s4.at[k], r4.at[k], {"sp": peer(k, -1)}
+        )
+
+    def pair_sum(i):
+        def start(k, carry):
+            side(k).start()
+            return carry
+
+        lax.fori_loop(i * per, i * per + per, start, 0)
+
+    def lane_sum(i):
+        def body(k, carry):
+            side(k).wait_recv()
+            for j in range(1, n_y):
+                y_to = wrapped(y + j, n_y)
+                send_b[j, rows(k), :] = (
+                    partial[rows(k), cols(y_to, core)].astype(f32)
+                    + recv_a[rows(k), sub(y_to)].astype(f32)
+                ).astype(bf16)
+                lane(k, j).start()
+            return carry
+
+        lax.fori_loop(i * per, i * per + per, body, 0)
+
+    def total(k):
+        summed = partial[rows(k), own].astype(f32) + recv_a[rows(k), sub(y)].astype(f32)
         for j in range(1, n_y):
-            along(k, j).start()
-        across(k, 0, core).start()
-
-    def second(k):
-        for j in range(1, n_y):
-            came = x.at[rows(wrapped(me - k, n_sp)), cols(wrapped(y - j, n_y), core)]
-            sent(came, came, s2.at[j, k], r2.at[j, k], other).wait_recv()
-            across(k, j, core).start()
-
-    forward(0)
-
-    def body(k, carry):
-        came = x.at[rows(wrapped(me - k, n_sp)), own]
-        sent(came, came, s1.at[k], r1.at[k], other).wait_recv()
-        forward(k)
-        second(k - 1)
+            lane(k, j).wait_recv()
+            summed = summed + recv_b[j, rows(k), :].astype(f32)
+        return summed.astype(bf16)
+
+    def go_home(i):
+        def body(k, carry):
+            send_c[rows(k), :] = total(k)
+            home(k).start()
+            return carry
+
+        lax.fori_loop(jnp.maximum(i * per, 1), i * per + per, body, 0)
+
+    hop_one(0)
+    hop_two(0)
+    for load in loads:
+        load.wait()
+
+    def stage(i, carry):
+        hop_one(i + 1)
+        hop_three(i)
+        compute(i)
+        pair_sum(i)
+        hop_two(i + 1)
+
+        @pl.when(i >= 1)
+        def _():
+            go_home(i - 1)
+
+        lane_sum(i)
         return carry
 
-    lax.fori_loop(1, n_sp, body, 0)
-    second(n_sp - 1)
-
-    def finish(k, carry):
-        for j in range(n_y):
-            across(k, j, 1 - core).wait_recv()
-            across(k, j, core).wait_send()
-        for j in range(1, n_y):
-            along(k, j).wait_send()
+    lax.fori_loop(0, chunks - 1, stage, 0)
+    hop_three(chunks - 1)
+    compute(chunks - 1)
+    pair_sum(chunks - 1)
+    if chunks > 1:
+        go_home(chunks - 2)
+    lane_sum(chunks - 1)
+    recv_c[rows(me), :] = total(0)
+    go_home(chunks - 1)
+
+    def finish_home(k, carry):
+        came = recv_c.at[rows(peer(k, 1))]
+        sent(came, came, s4.at[k], r4.at[k], other).wait_recv()
         return carry
 
-    lax.fori_loop(0, n_sp, finish, 0)
-
-    def finish_first(k, carry):
-        first(k).wait_send()
-        return carry
-
-    lax.fori_loop(1, n_sp, finish_first, 0)
-
-
-def combine_kernel(
-    n_sp, n_tp, partial, mix_hi, mix_lo, normed, gain, out,
-    recv_a, send_b, recv_b, send_c, recv_c, routed,
-    sa, ra, sb, rb, s1, r1, sy, ry, sc, rc,
-):
-    y, core = place(n_tp)
-    n_y = n_tp // 2
-    me = lax.axis_index("sp")
-    cap = partial.shape[0] // n_sp
-    features = partial.shape[1]
-    width, half = features // n_tp, features // 2
-    other = {"tp": y * 2 + 1 - core}
-
-    def cols(y_of, core_of):
-        return pl.ds(pl.multiple_of((core_of * n_y + y_of) * width, width), width)
-
-    def sub(y_of):
-        return pl.ds(pl.multiple_of(y_of * width, width), width)
-
-    def rows(block):
-        return pl.ds(pl.multiple_of(block * cap, cap), cap)
-
-    def block_of(k):
-        return wrapped(me + k + 1, n_sp)
-
-    greet(n_sp, n_tp)
-
-    def across(k):
-        at = rows(block_of(k))
-        far = pl.ds(pl.multiple_of((1 - core) * half, half), half)
-        return sent(partial.at[at, far], recv_a.at[at], sa.at[k], ra.at[k], other)
-
-    def along(k, j):
-        at = rows(block_of(k))
-        return sent(
-            send_b.at[j, at], recv_b.at[j, at], sb.at[j, k], rb.at[j, k],
-            {"tp": wrapped(y + j, n_y) * 2 + core},
-        )
-
-    def home(k):
-        to = block_of(k)
-        return sent(send_c.at[rows(to)], recv_c.at[rows(me)], s1.at[k], r1.at[k], {"sp": to})
-
-    def start_a(k, carry):
-        across(k).start()
-        return carry
-
-    lax.fori_loop(0, n_sp, start_a, 0)
-
-    def start_b(k, carry):
-        across(k).wait_recv()
-        at = rows(block_of(k))
-        for j in range(1, n_y):
-            y_to = wrapped(y + j, n_y)
-            send_b[j, at, :] = (
-                partial[at, cols(y_to, core)].astype(f32) + recv_a[at, sub(y_to)].astype(f32)
-            ).astype(bf16)
-            along(k, j).start()
-        return carry
-
-    lax.fori_loop(0, n_sp, start_b, 0)
-
-    def total(k):
-        at = rows(block_of(k))
-        summed = partial[at, cols(y, core)].astype(f32) + recv_a[at, sub(y)].astype(f32)
-        for j in range(1, n_y):
-            along(k, j).wait_recv()
-            summed = summed + recv_b[j, at, :].astype(f32)
-        return summed.astype(bf16)
-
-    def start_c(k, carry):
-        summed = total(k)
-        send_c[rows(block_of(k)), :] = summed
-        home(k).start()
-        return carry
-
-    lax.fori_loop(0, n_sp - 1, start_c, 0)
-    recv_c[rows(me), :] = total(n_sp - 1)
-
-    def finish_c(k, carry):
-        came = recv_c.at[rows(wrapped(me - k - 1, n_sp))]
-        sent(came, came, s1.at[k], r1.at[k], other).wait_recv()
-        home(k).wait_send()
-        return carry
-
-    lax.fori_loop(0, n_sp - 1, finish_c, 0)
-    routed[:, cols(y, core)] = (
+    lax.fori_loop(1, n_sp, finish_home, 0)
+    routed[:, own] = (
         jnp.dot(mix_hi[...], recv_c[...], preferred_element_type=f32)
         + jnp.dot(mix_lo[...], recv_c[...], preferred_element_type=f32)
     ).astype(bf16)
@@ -334,20 +348,34 @@
 
     lax.fori_loop(0, out.shape[0] // step, norm, 0)
 
+    def finish_sides(k, carry):
+        side(k).wait_send()
+        for j in range(1, n_y):
+            lane(k, j).wait_send()
+        return carry
+
+    lax.fori_loop(0, n_sp, finish_sides, 0)
+
     def finish(k, carry):
-        across(k).wait_send()
+        first(k).wait_send()
+        home(k).wait_send()
+        for j in range(n_y):
+            across(k, j, core).wait_send()
         for j in range(1, n_y):
             along(k, j).wait_send()
         return carry
 
-    lax.fori_loop(0, n_sp, finish, 0)
-
-
-def called(kernel, args, shape, scratch, number):
+    lax.fori_loop(1, n_sp, finish, 0)
+
+
+def called(kernel, args, shape, scratch, number, far=()):
     return pl.pallas_call(
         kernel,
         out_shape=jax.ShapeDtypeStruct(shape, bf16),
-        in_specs=[pl.BlockSpec(memory_space=pltpu.VMEM)] * len(args),
+        in_specs=[
+            pl.BlockSpec(memory_space=pl.ANY if n in far else pltpu.VMEM)
+            for n in range(len(args))
+        ],
         out_specs=pl.BlockSpec(memory_space=pltpu.VMEM),
         scratch_shapes=scratch,
         compiler_params=pltpu.CompilerParams(
@@ -373,29 +401,20 @@
     )
 
 
-def dispatch(select, normed, n_sp, n_tp):
-    slots, features = select.shape[0], normed.shape[1]
-    n_y = n_tp // 2
-    return called(
-        functools.partial(dispatch_kernel, n_sp, n_tp),
-        (select, normed),
-        (slots, features),
-        [pltpu.VMEM((slots, features // n_tp), bf16)]
-        + [DMA((n_sp,))] * 2
-        + [DMA((n_y, n_sp))] * 4,
-        1,
-    )
-
-
-def combine(partial, mix_hi, mix_lo, normed, gain, n_sp, n_tp):
-    slots, features = partial.shape
-    rows = normed.shape[0]
+def expert_layer(select, normed, w_gate, w_up, w_down, mix_hi, mix_lo, gain, n_sp, n_tp):
+    slots, (rows, features) = select.shape[0], normed.shape
     n_y, width = n_tp // 2, features // n_tp
     return called(
-        functools.partial(combine_kernel, n_sp, n_tp),
-        (partial, mix_hi, mix_lo, normed, gain.reshape(1, features)),
+        functools.partial(experts_kernel, n_sp, n_tp),
+        (select, normed, w_gate, w_up, w_down, mix_hi, mix_lo, gain.reshape(1, features)),
         (rows, features),
         [
+            pltpu.VMEM((slots, features), bf16),
+            pltpu.VMEM((slots, width), bf16),
+            pltpu.VMEM(w_gate.shape[1:], bf16),
+            pltpu.VMEM(w_up.shape[1:], bf16),
+            pltpu.VMEM(w_down.shape[1:], bf16),
+            pltpu.VMEM((slots, features), bf16),
             pltpu.VMEM((slots, features // 2), bf16),
             pltpu.VMEM((n_y, slots, width), bf16),
             pltpu.VMEM((n_y, slots, width), bf16),
@@ -403,11 +422,15 @@
             pltpu.VMEM((slots, width), bf16),
             pltpu.VMEM((rows, features), bf16),
         ]
+        + [DMA((3,))]
+        + [DMA((n_sp,))] * 2
+        + [DMA((n_y, n_sp))] * 4
         + [DMA((n_sp,))] * 2
         + [DMA((n_y, n_sp))] * 2
         + [DMA((n_sp,))] * 2
         + spread_sems(n_y),
-        2,
+        1,
+        far=(2, 3, 4),
     )
 
 
@@ -465,12 +488,9 @@
     mix_lo = (mix - mix_hi).astype(bf16)
     mix_hi = mix_hi.astype(bf16)
     normed = project(product, residual, mix_gain, n_tp)
-    flat_in = dispatch(select, normed, n_sp, n_tp)
-    gate_pre = jnp.dot(flat_in, w_gate[0], preferred_element_type=f32)
-    upper = jnp.dot(flat_in, w_up[0], preferred_element_type=f32)
-    hidden = (jax.nn.silu(gate_pre) * upper).astype(bf16)
-    partial_value = jnp.dot(hidden, w_down[0], preferred_element_type=f32).astype(bf16)
-    return combine(partial_value, mix_hi, mix_lo, normed, out_gain, n_sp, n_tp)
+    return expert_layer(
+        select, normed, w_gate, w_up, w_down, mix_hi, mix_lo, out_gain, n_sp, n_tp
+    )
 
 
 def solution(mesh):

time: 176 us -> 133 us (0.76)
  matrix products: 38.2 us -> 5.17 us
  Pallas kernels: 115 us -> 108 us
  other arithmetic: 7.91 us -> 5.6 us
    dot_general x2 -> x0, matrix products: 32.4 us -> none  [the longest x1 20.6 us: shards(): jnp.dot(hidden, w_down[0], preferred_element_type=f32).astype(bf16)]
    pallas_call x3 -> x2, Pallas kernels: 115 us -> 108 us  [called(): pl.pallas_call(kernel, out_shape=jax.ShapeDtypeStruct(shape, bf16), in_sp...]
  transfers between devices with their start and end apart: 2 -> 2, of which waited for: 0 -> 0; matrix products, arithmetic and copies ran while one was open for 5% -> 6% of each run, Pallas kernels for 0% -> 0%
where the time goes in v2:
time: 133 us
  Pallas kernels  108 us (81%)
  starting transfers between devices  8.3 us (6%)
  other arithmetic  5.6 us (4%)
  local copies, waits for them, and re-layouts  5.49 us (4%)
  matrix products  5.17 us (4%)
    pallas_call x2, Pallas kernels, called(): pl.pallas_call(kernel, out_shape=jax.ShapeDtypeStruct(shape, bf16), in_sp...  108 us
    ppermute x2, starting transfers between devices, passed_along(): lax.ppermute(value, axis, [(source, source + steps) for source in range(i...  8.3 us
    dot_general x1, matrix products, shards(): jnp.dot(mixed_rows, out_proj, preferred_element_type=f32).astype(bf16)  5.17 us
    unnamed x10, local copies, waits for them, and re-layouts  3.14 us
  transfers between devices with their start and end apart: 2, of which 0 were waited for; matrix products, arithmetic and copies ran while one was open for 6% of the time, Pallas kernels for 0%

profile of v2, /device:TPU:0, one launch (start us, length us, event | category | flops | bytes accessed | tf_op | source)
XLA Modules:
  0.0 132.5 jit_solution(10764206814115899602)
XLA Ops:
  0.0 0.0 copy-start
  0.0 0.9 slice.118
  0.9 4.9 %collective-permute-start.1 = (s32[15]{0:T(128)S(1)}, s32[15]{0:T(128)S(1)}, u32[]{:S(2)}, u32[]{:S(2)}) collective-permute-start(s32[15]{0:T(128)S(1)} %slice.118), channel_id=1, source_target_pairs={{0,4},{4,8},{8,12},{12,16},{16,20},{20,24},{24,28},{1,5},{5,9},{9,... | collective-permute-start | bytes 188 | tf_op jit(solution)/shard_map/ppermute | solution.py:23
  5.8 0.7 slice.116
  6.5 3.4 %collective-permute-start = (bf16[15,512]{1,0:T(8,128)(2,1)S(1)}, bf16[15,512]{1,0:T(8,128)(2,1)S(1)}, u32[]{:S(2)}, u32[]{:S(2)}) collective-permute-start(bf16[15,512]{1,0:T(8,128)(2,1)S(1)} %slice.116), channel_id=1, source_target_pairs={{0,4},{4,8},{8,12},{12,16},{16,20},{20,24},{24,28},{1,5},{5,9},{9,... | collective-permute-start | bytes 46088 | tf_op jit(solution)/shard_map/ppermute | solution.py:23
  10.1 0.8 copy.30
  10.9 0.1 eq.117
  11.1 0.0 copy-start.2
  11.1 0.0 copy-start.1
  11.1 0.1 eq.113
  11.3 1.1 reduce-window.6
  12.4 0.2 slice_reduce_fusion
  12.7 0.1 fusion.36
  12.8 0.1 reshape.118
  12.9 0.1 copy.32
  13.0 0.7 multiply_add_fusion
  13.7 0.0 copy-start.3
  13.7 1.1 select_reduce_fusion
  14.8 1.2 fusion
  16.0 1.0 fusion.2.select
  17.0 0.0 collective-permute-done.1
  17.0 0.0 copy-done.2
  17.0 0.1 pad_add_fusion
  17.0 0.1 compare_and_fusion.14
  17.1 0.0 collective-permute-done
  17.2 0.0 copy-done.1
  17.2 0.1 maximum_convert_fusion
  17.2 0.0 copy-done
  17.3 0.0 copy-done.3
  17.3 5.2 %convolution_convert_fusion.proj = bf16[256,2048]{1,0:T(8,128)(2,1)} fusion(bf16[512,2048]{1,0:T(8,128)(2,1)S(1)} %copy-done, f32[271,512]{1,0:T(8,128)S(1)} %maximum_convert_fusion, f32[512]{0:T(512)S(1)} %copy-done.3, pred[512]{0:T(512)(128)(4,1)S(1)} %get-tuple-element.24, pred[512]{0:T(512)(128)(4,1)S(1)} %get-tuple-element.25, ...), kind=kOutput, calls=%fused_computation | convolution fusion | flops 548143104 | bytes 11552768 | tf_op jit(solution)/shard_map/dot_general | solution.py:474
  22.4 21.1 %shard_map.118.normed = bf16[256,2048]{1,0:T(8,128)(2,1)} custom-call(bf16[256,2048]{1,0:T(8,128)(2,1)} %convolution_convert_fusion.proj, bf16[256,2048]{1,0:T(8,128)(2,1)} %residual.1, f32[1,2048]{1,0:T(1,128)} %bitcast.13), custom_call_target="tpu_custom_call" | custom-call | tf_op jit(solution)/shard_map/pallas_call | solution.py:372
  43.6 86.6 %shard_map.119 = bf16[256,2048]{1,0:T(8,128)(2,1)} custom-call(bf16[1024,256]{1,0:T(8,128)(2,1)} %fusion.2.select, bf16[256,2048]{1,0:T(8,128)(2,1)} %shard_map.118.normed, bf16[1,2048,1408]{2,1,0:T(8,128)(2,1)} %w_gate.1, bf16[1,2048,1408]{2,1,0:T(8,128)(2,1)} %w_up.1, bf16[1,1408,2048]{2,1,0:T(8,128)(2,1)} %w_down.1, ...), custom_call_target="tpu_custom_call" | custom-call | tf_op jit(solution)/shard_map/pallas_call | solution.py:372
  130.2 2.3 %copy.34 = bf16[256,2048]{1,0:T(8,128)(2,1)} copy(bf16[256,2048]{1,0:T(8,128)(2,1)} %shard_map.119) | data formatting | bytes 2097152
  (12 shorter events, 0.2 us)
Async XLA Ops:
  0.0 17.2 %copy-start = (bf16[512,2048]{1,0:T(8,128)(2,1)S(1)}, bf16[512,2048]{1,0:T(8,128)(2,1)}, u32[]{:S(2)}) copy-start(bf16[512,2048]{1,0:T(8,128)(2,1)} %param.15) | copy-start | bytes 6291460
  0.9 16.1 %collective-permute-start.1 = (s32[15]{0:T(128)S(1)}, s32[15]{0:T(128)S(1)}, u32[]{:S(2)}, u32[]{:S(2)}) collective-permute-start(s32[15]{0:T(128)S(1)} %slice.118), channel_id=1, source_target_pairs={{0,4},{4,8},{8,12},{12,16},{16,20},{20,24},{24,28},{1,5},{5,9},{9,... | collective-permute-start | bytes 188 | tf_op jit(solution)/shard_map/ppermute | solution.py:23
  6.5 10.6 %collective-permute-start = (bf16[15,512]{1,0:T(8,128)(2,1)S(1)}, bf16[15,512]{1,0:T(8,128)(2,1)S(1)}, u32[]{:S(2)}, u32[]{:S(2)}) collective-permute-start(bf16[15,512]{1,0:T(8,128)(2,1)S(1)} %slice.116), channel_id=1, source_target_pairs={{0,4},{4,8},{8,12},{12,16},{16,20},{20,24},{24,28},{1,5},{5,9},{9,... | collective-permute-start | bytes 46088 | tf_op jit(solution)/shard_map/ppermute | solution.py:23
  11.1 5.9 %copy-start.2 = (s32[256]{0:T(256)S(1)}, s32[256]{0:T(256)}, u32[]{:S(2)}) copy-start(s32[256]{0:T(256)} %param.13) | copy-start | bytes 3076
  11.1 6.1 %copy-start.1 = (bf16[256,512]{1,0:T(8,128)(2,1)S(1)}, bf16[256,512]{1,0:T(8,128)(2,1)}, u32[]{:S(2)}) copy-start(bf16[256,512]{1,0:T(8,128)(2,1)} %param.12) | copy-start | bytes 786436
  13.7 3.6 %copy-start.3 = (f32[512]{0:T(512)S(1)}, f32[512]{0:T(512)}, u32[]{:S(2)}) copy-start(f32[512]{0:T(512)} %param.14) | copy-start | bytes 6148

commit v3 on v2

--- a/solution.py
+++ b/solution.py
@@ -17,24 +17,11 @@
 pool_reach = 15
 
 
-def passed_along(value, axis, steps):
-    count = lax.axis_size(axis)
-    initial, last = (max(0, -steps), min(count, count - steps))
-    return lax.ppermute(value, axis, [(source, source + steps) for source in range(initial, last)])
-
-
 def layer_norm(summed, norm_gain):
     row_mean = jnp.mean(summed, axis=-1, keepdims=True)
     centred = summed - row_mean
     row_var = jnp.mean(centred * centred, axis=-1, keepdims=True)
     return centred * lax.rsqrt(row_var + norm_eps) * norm_gain
-
-
-def pair_slots(pair_ids, experts):
-    flat_ids = pair_ids.reshape(-1)
-    onehot = (flat_ids[:, None] == jnp.arange(experts, dtype=jnp.int32)[None, :]).astype(jnp.int32)
-    before = jnp.cumsum(onehot, axis=0) - onehot
-    return jnp.sum(before * onehot, axis=1).reshape(pair_ids.shape)
 
 
 def wrapped(value, count):
@@ -107,50 +94,76 @@
         copy.wait_send()
 
 
-def project_kernel(
-    n_tp, proj, residual, gain, normed, recv_a, send_b, recv_b, sa, ra, sb, rb, sy, ry, sc, rc
-):
-    y, core = place(n_tp)
-    n_y = n_tp // 2
-    share = proj.shape[0] // n_tp
-    other = {"tp": y * 2 + 1 - core}
-
-    def rows(y_of, core_of):
-        return pl.ds(pl.multiple_of((core_of * n_y + y_of) * share, share), share)
-
-    greet(1, n_tp)
-    halves = {}
-    for j in list(range(1, n_y)) + [0]:
-        y_to = wrapped(y + j, n_y)
-        halves[j] = sent(
-            proj.at[rows(y_to, 1 - core)], recv_a.at[j], sa.at[j], ra.at[j], other
-        )
-        halves[j].start()
-    along = []
-    for j in range(1, n_y):
-        y_to = wrapped(y + j, n_y)
-        halves[j].wait_recv()
-        send_b[j] = (proj[rows(y_to, core), :].astype(f32) + recv_a[j].astype(f32)).astype(bf16)
-        copy = sent(
-            send_b.at[j], recv_b.at[j], sb.at[j], rb.at[j], {"tp": y_to * 2 + core}
-        )
-        copy.start()
-        along.append(copy)
-    halves[0].wait_recv()
-    summed = proj[rows(y, core), :].astype(f32) + recv_a[0].astype(f32)
-    summed = summed + alpha_res * residual[rows(y, core), :].astype(f32)
-    for j in range(1, n_y):
-        along[j - 1].wait_recv()
-        summed = summed + recv_b[j].astype(f32)
-    normed[rows(y, core), :] = layer_norm(summed, gain[...]).astype(bf16)
-    spread(n_y, y, core, lambda a, b: normed.at[rows(a, b)], (sy, ry, sc, rc))
-    for copy in list(halves.values()) + along:
-        copy.wait_send()
-
-
-def experts_kernel(
-    n_sp, n_tp, select, normed, w_gate, w_up, w_down, mix_hi, mix_lo, gain, out,
+def pooled(n_sp, mixer, doc, scale, halo, halo_doc, ext, ext_doc, features):
+    tok_rows, chan_cols = mixer.shape
+    reach = pool_reach + 1
+    ext[pl.ds(0, reach), :] = halo[...].astype(f32)
+    ext[pl.ds(reach, tok_rows), :] = mixer[...].astype(f32)
+    ext_doc[pl.ds(0, reach), :] = halo_doc[...]
+    ext_doc[pl.ds(reach, tok_rows), :] = doc[...]
+    lanes = doc.shape[1]
+    position = lax.axis_index("sp") * tok_rows + lax.broadcasted_iota(
+        jnp.int32, (tok_rows, lanes), 0
+    )
+    length = jnp.ones((tok_rows, lanes), f32)
+    for lag in range(1, reach):
+        same = (ext_doc[pl.ds(reach - lag, tok_rows), :] == doc[...]) & (position >= lag)
+        length = length + jnp.where(same, 1.0, 0.0)
+    parts = []
+    for start in range(0, chan_cols, lanes):
+        at = pl.ds(start, lanes)
+        channel = lax.axis_index("tp") * chan_cols + start
+        channel = channel + lax.broadcasted_iota(jnp.int32, (1, lanes), 1)
+        window = jnp.where(channel < features // 4, 2.0, 4.0)
+        window = jnp.where(channel < features // 2, window, 8.0)
+        window = jnp.where(channel < features // 4 * 3, window, 16.0)
+        count = jnp.minimum(window, length)
+        own = ext[pl.ds(reach, tok_rows), at]
+        summed = own
+        for lag in range(1, reach):
+            shifted = ext[pl.ds(reach - lag, tok_rows), at]
+            summed = summed + jnp.where(count > lag, shifted, 0.0)
+        parts.append(((summed / count - own) * scale[:, start : start + lanes]).astype(bf16))
+    return jnp.concatenate(parts, axis=1) if len(parts) > 1 else parts[0]
+
+
+def over_slots(mix, rows):
+    return lax.dot_general(mix, rows, (((0,), (0,)), ((), ())), preferred_element_type=f32)
+
+
+def tables(ids, weights, select, mix_hi, mix_lo, experts):
+    tok_rows = ids.shape[1]
+    cap = select.shape[0] // experts
+    name = lax.broadcasted_iota(jnp.int32, (experts, tok_rows), 0)
+    zero_hot, one_hot = name == ids[0:1, :], name == ids[1:2, :]
+    hot = jnp.where(zero_hot | one_hot, 1.0, 0.0)
+    earlier = jnp.where(
+        lax.broadcasted_iota(jnp.int32, (tok_rows, tok_rows), 0)
+        < lax.broadcasted_iota(jnp.int32, (tok_rows, tok_rows), 1),
+        1.0,
+        0.0,
+    ).astype(bf16)
+    rank = jnp.dot(hot.astype(bf16), earlier, preferred_element_type=f32)
+    rank = jnp.where(hot > 0.0, rank, -1.0)
+    share = jnp.where(zero_hot, weights[0:1, :], jnp.where(one_hot, weights[1:2, :], 0.0))
+    high = share.astype(bf16).astype(f32)
+    low = share - high
+    slot = lax.broadcasted_iota(jnp.int32, (cap, tok_rows), 0).astype(f32)
+    for e in range(experts):
+        at = pl.ds(e * cap, cap)
+        same = slot == rank[e : e + 1, :]
+        select[at, :] = jnp.where(same, 1.0, 0.0).astype(bf16)
+        mix_hi[at, :] = jnp.where(same, high[e : e + 1, :], 0.0).astype(bf16)
+        mix_lo[at, :] = jnp.where(same, low[e : e + 1, :], 0.0).astype(bf16)
+
+
+def layer_kernel(
+    n_sp, n_tp, mixer, doc, scale, out_proj, residual, mix_gain, ids, weights,
+    w_gate, w_up, w_down, gain, out,
+    halo, halo_doc, ext, ext_doc, mixed, proj, half_in, half_out, share_in,
+    normed, select, mix_hi, mix_lo,
     x, send, gate_v, up_v, down_v, partial, recv_a, send_b, recv_b, send_c, recv_c, routed,
+    sh, rh, pa, qa, pb, qb, py, qy, pc, qc,
     sw, s1, r1, s2, r2, s3, r3, sa, ra, sb, rb, s4, r4, sy, ry, sc, rc,
 ):
     y, core = place(n_tp)
@@ -188,6 +201,60 @@
         load.start()
     greet(n_sp, n_tp)
 
+    tok_rows = mixer.shape[0]
+    reach = pool_reach + 1
+    last = pl.ds(tok_rows - reach, reach)
+    onward = {"sp": wrapped(me + 1, n_sp)}
+    halos = [
+        sent(mixer.at[last], halo, sh.at[0], rh.at[0], onward),
+        sent(doc.at[last], halo_doc, sh.at[1], rh.at[1], onward),
+    ]
+    for copy in halos:
+        copy.start()
+    tables(ids, weights, select, mix_hi, mix_lo, n_sp)
+    for copy in halos:
+        copy.wait_recv()
+    mixed[...] = pooled(n_sp, mixer, doc, scale, halo, halo_doc, ext, ext_doc, features)
+
+    share = tok_rows // n_tp
+
+    def held(y_of, core_of):
+        return pl.ds(pl.multiple_of((core_of * n_y + y_of) * share, share), share)
+
+    def multiply(core_of):
+        at = pl.ds(pl.multiple_of(core_of * (tok_rows // 2), tok_rows // 2), tok_rows // 2)
+        proj[at, :] = jnp.dot(
+            mixed[at, :], out_proj[...], preferred_element_type=f32
+        ).astype(bf16)
+
+    multiply(1 - core)
+    halves = {}
+    for j in list(range(1, n_y)) + [0]:
+        halves[j] = sent(
+            proj.at[held(wrapped(y + j, n_y), 1 - core)], half_in.at[j], pa.at[j], qa.at[j], other
+        )
+        halves[j].start()
+    multiply(core)
+    shares = []
+    for j in range(1, n_y):
+        halves[j].wait_recv()
+        half_out[j] = (
+            proj[held(wrapped(y + j, n_y), core), :].astype(f32) + half_in[j].astype(f32)
+        ).astype(bf16)
+        copy = sent(half_out.at[j], share_in.at[j], pb.at[j], qb.at[j], along_tp(j))
+        copy.start()
+        shares.append(copy)
+    halves[0].wait_recv()
+    projected = proj[held(y, core), :].astype(f32) + half_in[0].astype(f32)
+    projected = projected + alpha_res * residual[held(y, core), :].astype(f32)
+    for j in range(1, n_y):
+        shares[j - 1].wait_recv()
+        projected = projected + share_in[j].astype(f32)
+    normed[held(y, core), :] = layer_norm(projected, mix_gain[...]).astype(bf16)
+    spread(n_y, y, core, lambda a, b: normed.at[held(a, b)], (py, qy, pc, qc))
+    for copy in list(halves.values()) + shares + halos:
+        copy.wait_send()
+
     def first(k):
         to = peer(k, 1)
         return sent(send.at[rows(k)], x.at[rows(k), own], s1.at[k], r1.at[k], {"sp": to})
@@ -334,8 +401,7 @@
 
     lax.fori_loop(1, n_sp, finish_home, 0)
     routed[:, own] = (
-        jnp.dot(mix_hi[...], recv_c[...], preferred_element_type=f32)
-        + jnp.dot(mix_lo[...], recv_c[...], preferred_element_type=f32)
+        over_slots(mix_hi[...], recv_c[...]) + over_slots(mix_lo[...], recv_c[...])
     ).astype(bf16)
     spread(n_y, y, core, lambda a, b: routed.at[:, cols(a, b)], (sy, ry, sc, rc))
     step = 64
@@ -388,52 +454,6 @@
     return [DMA((n_y,))] * 4
 
 
-def project(proj, residual, gain, n_tp):
-    rows, features = proj.shape
-    n_y, share = n_tp // 2, rows // n_tp
-    piece = pltpu.VMEM((n_y, share, features), bf16)
-    return called(
-        functools.partial(project_kernel, n_tp),
-        (proj, residual, gain.reshape(1, features)),
-        (rows, features),
-        [piece] * 3 + [DMA((n_y,))] * 4 + spread_sems(n_y),
-        0,
-    )
-
-
-def expert_layer(select, normed, w_gate, w_up, w_down, mix_hi, mix_lo, gain, n_sp, n_tp):
-    slots, (rows, features) = select.shape[0], normed.shape
-    n_y, width = n_tp // 2, features // n_tp
-    return called(
-        functools.partial(experts_kernel, n_sp, n_tp),
-        (select, normed, w_gate, w_up, w_down, mix_hi, mix_lo, gain.reshape(1, features)),
-        (rows, features),
-        [
-            pltpu.VMEM((slots, features), bf16),
-            pltpu.VMEM((slots, width), bf16),
-            pltpu.VMEM(w_gate.shape[1:], bf16),
-            pltpu.VMEM(w_up.shape[1:], bf16),
-            pltpu.VMEM(w_down.shape[1:], bf16),
-            pltpu.VMEM((slots, features), bf16),
-            pltpu.VMEM((slots, features // 2), bf16),
-            pltpu.VMEM((n_y, slots, width), bf16),
-            pltpu.VMEM((n_y, slots, width), bf16),
-            pltpu.VMEM((slots, width), bf16),
-            pltpu.VMEM((slots, width), bf16),
-            pltpu.VMEM((rows, features), bf16),
-        ]
-        + [DMA((3,))]
-        + [DMA((n_sp,))] * 2
-        + [DMA((n_y, n_sp))] * 4
-        + [DMA((n_sp,))] * 2
-        + [DMA((n_y, n_sp))] * 2
-        + [DMA((n_sp,))] * 2
-        + spread_sems(n_y),
-        1,
-        far=(2, 3, 4),
-    )
-
-
 def shards(
     mixer_in,
     doc_ids,
@@ -448,48 +468,74 @@
     w_down,
     out_gain,
 ):
-    tok_rows, chan_cols = mixer_in.shape
+    n_sp, n_tp = lax.axis_size("sp"), lax.axis_size("tp")
+    n_y = n_tp // 2
+    rows, chan_cols = mixer_in.shape
     features = mix_gain.shape[0]
-    tail_rows = (mixer_in[tok_rows - pool_reach :], doc_ids[tok_rows - pool_reach :])
-    before_vals, before_doc = passed_along((tail_rows[0], tail_rows[1]), "sp", 1)
-    extended = jnp.concatenate([before_vals, mixer_in], axis=0).astype(jnp.float32)
-    extended_doc = jnp.concatenate([before_doc, doc_ids], axis=0)
-    positions = lax.axis_index("sp") * tok_rows + jnp.arange(tok_rows, dtype=jnp.int32)
-    channel = lax.axis_index("tp") * chan_cols + jnp.arange(chan_cols, dtype=jnp.int32)
-    window = jnp.left_shift(jnp.int32(2), channel // (features // 4))
-    window_sum = jnp.zeros((tok_rows, chan_cols), jnp.float32)
-    window_count = jnp.zeros((tok_rows, chan_cols), jnp.float32)
-    for lag_step in range(pool_reach + 1):
-        shifted = extended[pool_reach - lag_step : pool_reach - lag_step + tok_rows]
-        same_doc = (
-            extended_doc[pool_reach - lag_step : pool_reach - lag_step + tok_rows] == doc_ids
-        ) & (positions >= lag_step)
-        in_window = (same_doc[:, None] & (lag_step < window)[None, :]).astype(jnp.float32)
-        window_sum = window_sum + in_window * shifted
-        window_count = window_count + in_window
-    mixed_rows = ((window_sum / window_count - extended[pool_reach:]) * mix_scale).astype(
-        jnp.bfloat16
-    )
-    n_sp, n_tp = lax.axis_size("sp"), lax.axis_size("tp")
-    product = jnp.dot(mixed_rows, out_proj, preferred_element_type=f32).astype(bf16)
-    experts = n_sp
-    capacity = 4 * tok_rows // experts
-    ranks = pair_slots(expert_ids, experts)
-    target = expert_ids * capacity + ranks
-    slot_ids = jnp.arange(experts * capacity, dtype=jnp.int32)
-    select = (
-        (target[None, :, 0] == slot_ids[:, None]) | (target[None, :, 1] == slot_ids[:, None])
-    ).astype(bf16)
-    mix = jnp.sum(
-        jnp.where(target[:, :, None] == slot_ids[None, None, :], expert_weight[:, :, None], 0.0),
-        axis=1,
-    )
-    mix_hi = lax.reduce_precision(mix, 8, 7)
-    mix_lo = (mix - mix_hi).astype(bf16)
-    mix_hi = mix_hi.astype(bf16)
-    normed = project(product, residual, mix_gain, n_tp)
-    return expert_layer(
-        select, normed, w_gate, w_up, w_down, mix_hi, mix_lo, out_gain, n_sp, n_tp
+    width = features // n_tp
+    slots = 4 * rows // n_sp * n_sp
+    reach = pool_reach + 1
+    lanes = 128
+
+    def vmem(*shape):
+        return pltpu.VMEM(shape, bf16)
+
+    return called(
+        functools.partial(layer_kernel, n_sp, n_tp),
+        (
+            mixer_in,
+            jnp.broadcast_to(doc_ids[:, None], (rows, lanes)),
+            mix_scale.reshape(1, chan_cols),
+            out_proj,
+            residual,
+            mix_gain.reshape(1, features),
+            expert_ids.T,
+            expert_weight.T,
+            w_gate,
+            w_up,
+            w_down,
+            out_gain.reshape(1, features),
+        ),
+        (rows, features),
+        [
+            vmem(reach, chan_cols),
+            pltpu.VMEM((reach, lanes), jnp.int32),
+            pltpu.VMEM((rows + reach, chan_cols), f32),
+            pltpu.VMEM((rows + reach, lanes), jnp.int32),
+            vmem(rows, chan_cols),
+            vmem(rows, features),
+            vmem(n_y, rows // n_tp, features),
+            vmem(n_y, rows // n_tp, features),
+            vmem(n_y, rows // n_tp, features),
+            vmem(rows, features),
+            vmem(slots, rows),
+            vmem(slots, rows),
+            vmem(slots, rows),
+            vmem(slots, features),
+            vmem(slots, width),
+            vmem(*w_gate.shape[1:]),
+            vmem(*w_up.shape[1:]),
+            vmem(*w_down.shape[1:]),
+            vmem(slots, features),
+            vmem(slots, features // 2),
+            vmem(n_y, slots, width),
+            vmem(n_y, slots, width),
+            vmem(slots, width),
+            vmem(slots, width),
+            vmem(rows, features),
+        ]
+        + [DMA((2,))] * 2
+        + [DMA((n_y,))] * 4
+        + spread_sems(n_y)
+        + [DMA((3,))]
+        + [DMA((n_sp,))] * 2
+        + [DMA((n_y, n_sp))] * 4
+        + [DMA((n_sp,))] * 2
+        + [DMA((n_y, n_sp))] * 2
+        + [DMA((n_sp,))] * 2
+        + spread_sems(n_y),
+        0,
+        far=(8, 9, 10),
     )
 
 

time: 133 us -> 125 us (0.940)
  Pallas kernels: 108 us -> 121 us
  starting transfers between devices: 8.3 us -> 0 us
  other arithmetic: 5.6 us -> 0 us
  matrix products: 5.17 us -> 0 us
  local copies, waits for them, and re-layouts: 5.49 us -> 3.74 us
    pallas_call x2 -> x1, Pallas kernels: 108 us -> 121 us  [called(): pl.pallas_call(kernel, out_shape=jax.ShapeDtypeStruct(shape, bf16), in_sp...]
    ppermute x2 -> x0, starting transfers between devices: 8.3 us -> none  [passed_along(): lax.ppermute(value, axis, [(source, source + steps) for source in range(i...]
    dot_general x1 -> x0, matrix products: 5.17 us -> none  [shards(): jnp.dot(mixed_rows, out_proj, preferred_element_type=f32).astype(bf16)]
    convert_element_type x4 -> x0, other arithmetic: 2.29 us -> none  [the longest x1 1.21 us: shards(): mix_lo = (mix - mix_hi).astype(bf16)]
    slice x4 -> x0, local copies, waits for them, and re-layouts: 1.85 us -> none  [the longest x1 0.9 us: shards(): doc_ids[tok_rows - pool_reach:]]
    broadcast_in_dim x0 -> x1, local copies, waits for them, and re-layouts: none -> 1.43 us  [shards(): jnp.broadcast_to(doc_ids[:, None], (rows, lanes))]
    unnamed x10 -> x1, local copies, waits for them, and re-layouts: 3.14 us -> 2.3 us
  transfers between devices with their start and end apart: 2 -> 0, of which waited for: 0 -> 0; matrix products, arithmetic and copies ran while one was open for 6% -> 0% of each run, Pallas kernels for 0% -> 0%
where the time goes in v3:
time: 125 us
  Pallas kernels  121 us (97%)
  local copies, waits for them, and re-layouts  3.74 us (3%)
    pallas_call x1, Pallas kernels, called(): pl.pallas_call(kernel, out_shape=jax.ShapeDtypeStruct(shape, bf16), in_sp...  121 us

profile of v3, /device:TPU:0, one launch (start us, length us, event | category | flops | bytes accessed | tf_op | source)
XLA Modules:
  0.0 125.0 jit_solution(8784266230009957348)
XLA Ops:
  0.0 1.4 %broadcast_in_dim.2.doc = s32[256,128]{1,0:T(8,128)} broadcast(s32[256]{0:T(256)} %param.13), dimensions={0} | broadcast | bytes 132096 | tf_op jit(solution)/shard_map/broadcast_in_dim | solution.py:487
  1.4 121.2 %shard_map.118 = bf16[256,2048]{1,0:T(8,128)(2,1)} custom-call(bf16[256,512]{1,0:T(8,128)(2,1)} %mixer.1, s32[256,128]{1,0:T(8,128)} %broadcast_in_dim.2.doc, f32[1,512]{1,0:T(1,128)} %bitcast.7, bf16[512,2048]{1,0:T(8,128)(2,1)} %out_proj.1, bf16[256,2048]{1,0:T(8,128)(2,1)} %residual.1, f32[1,2048]{1,0:T(1,128)} %bitcast.5, s32[2,256]{1,0:T(2,128)} %bitcast.8, ...), custom_call_target="tpu_custom_call" | custom-call | tf_op jit(solution)/shard_map/pallas_call | solution.py:438
  122.7 2.3 %copy.14 = bf16[256,2048]{1,0:T(8,128)(2,1)} copy(bf16[256,2048]{1,0:T(8,128)(2,1)} %shard_map.118) | data formatting | bytes 2097152

commit v4 on v3

--- a/solution.py
+++ b/solution.py
@@ -172,7 +172,7 @@
     cap = select.shape[0] // n_sp
     features = normed.shape[1]
     width, half = features // n_tp, features // 2
-    per = max(1, min(n_sp, 256 // cap))
+    per = max(1, min(n_sp, 128 // cap))
     chunks = n_sp // per
     other = {"tp": y * 2 + 1 - core}
 
@@ -367,30 +367,34 @@
 
     hop_one(0)
     hop_two(0)
+    if chunks > 1:
+        hop_one(1)
     for load in loads:
         load.wait()
 
     def stage(i, carry):
-        hop_one(i + 1)
+        @pl.when(i + 2 < chunks)
+        def _():
+            hop_one(i + 2)
+
         hop_three(i)
         compute(i)
         pair_sum(i)
-        hop_two(i + 1)
-
-        @pl.when(i >= 1)
+
+        @pl.when(i + 1 < chunks)
         def _():
-            go_home(i - 1)
+            hop_two(i + 1)
+
+        @pl.when(i >= 2)
+        def _():
+            go_home(i - 2)
 
         lane_sum(i)
         return carry
 
-    lax.fori_loop(0, chunks - 1, stage, 0)
-    hop_three(chunks - 1)
-    compute(chunks - 1)
-    pair_sum(chunks - 1)
+    lax.fori_loop(0, chunks, stage, 0)
     if chunks > 1:
         go_home(chunks - 2)
-    lane_sum(chunks - 1)
     recv_c[rows(me), :] = total(0)
     go_home(chunks - 1)
 

time: 125 us -> 112 us (0.90)
  Pallas kernels: 121 us -> 108 us
    pallas_call x1, Pallas kernels: 121 us -> 108 us  [called(): pl.pallas_call(kernel, out_shape=jax.ShapeDtypeStruct(shape, bf16), in_sp...]
where the time goes in v4:
time: 112 us
  Pallas kernels  108 us (96%)
  local copies, waits for them, and re-layouts  3.74 us (3%)
    pallas_call x1, Pallas kernels, called(): pl.pallas_call(kernel, out_shape=jax.ShapeDtypeStruct(shape, bf16), in_sp...  108 us
    unnamed x1, local copies, waits for them, and re-layouts  2.3 us

profile of v4, /device:TPU:0, one launch (start us, length us, event | category | flops | bytes accessed | tf_op | source)
XLA Modules:
  0.0 111.7 jit_solution(1358861875425063372)
XLA Ops:
  0.0 1.4 %broadcast_in_dim.2.doc = s32[256,128]{1,0:T(8,128)} broadcast(s32[256]{0:T(256)} %param.13), dimensions={0} | broadcast | bytes 132096 | tf_op jit(solution)/shard_map/broadcast_in_dim | solution.py:491
  1.4 108.0 %shard_map.118 = bf16[256,2048]{1,0:T(8,128)(2,1)} custom-call(bf16[256,512]{1,0:T(8,128)(2,1)} %mixer.1, s32[256,128]{1,0:T(8,128)} %broadcast_in_dim.2.doc, f32[1,512]{1,0:T(1,128)} %bitcast.7, bf16[512,2048]{1,0:T(8,128)(2,1)} %out_proj.1, bf16[256,2048]{1,0:T(8,128)(2,1)} %residual.1, f32[1,2048]{1,0:T(1,128)} %bitcast.5, s32[2,256]{1,0:T(2,128)} %bitcast.8, ...), custom_call_target="tpu_custom_call" | custom-call | tf_op jit(solution)/shard_map/pallas_call | solution.py:442
  109.4 2.3 %copy.14 = bf16[256,2048]{1,0:T(8,128)(2,1)} copy(bf16[256,2048]{1,0:T(8,128)(2,1)} %shard_map.118) | data formatting | bytes 2097152
